TPU v7x, 32 devices: a whole 2x2x4 slice. The times are simulated.
32 devices in a mesh: sp: 8 (over z, y), tp: 4 (over x, core).
Axes of the slice: x: 2, y: 2, z: 4, core: 2. Of those that a mesh axis runs over, the one named last changes fastest.
Arguments:
- latents: bfloat16 [2048, 4096], P('sp'), may hold values from -0.4375 to 0.4375
- query_heads: bfloat16 [2048, 16, 128], P('sp', 'tp'), may hold values from -8 to 8
- key_heads: bfloat16 [2048, 16, 128], P('sp', 'tp'), may hold values from -8 to 8
- value_heads: bfloat16 [2048, 16, 128], P('sp', 'tp'), may hold values from -6 to 6
- map_outputs: bfloat16 [2048, 2, 16, 128], P('sp', None, 'tp'), may hold values from -6 to 6
- log_sums: float32 [2048, 16, 2], P('sp', 'tp'), may hold values from -600 to 600, as said below
- out_grad: bfloat16 [2048, 16, 128], P('sp', 'tp'), may hold values from -6 to 6
- mix_lambda: float32 [16], P('tp'), may hold values from 0.3 to 0.8
- norm_gain: float32 [128], replicated, may hold values from 0.1 to 1.9
Outputs:
- query_grad: bfloat16 [2048, 16, 128], P('sp', 'tp')
- key_grad: bfloat16 [2048, 16, 128], P('sp', 'tp')
- value_grad: bfloat16 [2048, 16, 128], P('sp', 'tp')
- weight_grad: float32 [4096, 2048], P('sp', 'tp')
Inputs may be any that keep to these rules, and one draw needn't show every extreme that they name: query_heads, key_heads and value_heads together with map_outputs and log_sums are one consistent causal forward pass: log_sums is the row's log-sum of exp(score_m) over keys at or before the row, and map_outputs[:, m] is prob_m times value_heads rounded to bfloat16.
All inputs are finite; a program needn't handle non-finite values.
Results may differ from a plain program's by a relative error of at most 0.019.
Values may be sent and summed in bfloat16 or wider, within the bound.
A program may use at most 64 MiB of HBM per device.

v0:
```python
import functools
import math

import jax
import jax.numpy as jnp
from jax import lax
from jax.experimental import pallas as pl
from jax.experimental.pallas import tpu as pltpu
from jax.sharding import PartitionSpec as P

EPSILON = 1e-05
LOG2E = math.log2(math.e)
F32 = jnp.float32
BF16 = jnp.bfloat16
MESH = pl.DeviceIdType.MESH


def dot_nn(a, b):
    return lax.dot_general(a, b, (((1,), (0,)), ((), ())), preferred_element_type=F32)


def dot_nt(a, b):
    return lax.dot_general(a, b, (((1,), (1,)), ((), ())), preferred_element_type=F32)


def dot_tn(a, b):
    return lax.dot_general(a, b, (((0,), (0,)), ((), ())), preferred_element_type=F32)


def norm_backward(heads, width, lam_ref, gain_ref, mo_ref, og_ref, lse_ref, grad_ref, col_ref, row_ref):
    for h in range(heads):
        first = mo_ref[:, 0, h, :].astype(F32)
        second = mo_ref[:, 1, h, :].astype(F32)
        lam = lam_ref[h]
        combined = first - lam * second
        inverse = lax.rsqrt(jnp.mean(combined * combined, axis=-1, keepdims=True) + EPSILON)
        weighted = gain_ref[...] * og_ref[:, h, :].astype(F32)
        grad = (
            inverse * weighted
            - inverse**3 * combined * jnp.mean(combined * weighted, axis=-1, keepdims=True)
        ).astype(BF16)
        grad_ref[:, h * width : (h + 1) * width] = grad
        wide = grad.astype(F32)
        lse = lse_ref[h] * LOG2E
        log_lam = jnp.log(jnp.full((1, 1), lam, F32)) * LOG2E
        lane = lax.broadcasted_iota(jnp.int32, wide.shape, 1)
        stats = jnp.where(lane == 0, lse[:, 0:1], lse[:, 1:2] - log_lam)
        stats = jnp.where(lane == 2, jnp.sum(wide * first, axis=-1, keepdims=True), stats)
        stats = jnp.where(lane == 3, jnp.sum(wide * second, axis=-1, keepdims=True), stats)
        col_ref[h] = stats
        row_ref[h] = jnp.transpose(stats)[0:4]


def main_kernel(nsp, ntp, heads, width, lam, gain, lat, own_k, own_v, own_q, mo, og, lse,
                dq_out, dk_out, dv_out, wg_out,
                own_g, col, row, own_dq, kvb, qgb, stb, dqb, latb, dq_acc, dk_acc, dv_acc,
                kv_s, qg_s, st_s, dq_s, kv_r, qg_r, st_r, dq_r,
                la_s, la_r, lb_s, lb_r, own_sem):
    nz = nsp // 2
    s = lax.axis_index("sp")
    t = lax.axis_index("tp")
    z, y = s // 2, lax.rem(s, 2)
    rows = own_k.shape[0]
    part = rows // ntp
    slab = lat.shape[1] // nsp
    score_scale = (width // 2) ** (-0.5)
    exp_scale = score_scale * LOG2E

    barrier = pltpu.get_barrier_semaphore()
    for d in range(1, nsp):
        pl.semaphore_signal(barrier, inc=1, device_id={"sp": lax.rem(s + d, nsp)}, device_id_type=MESH)
    for d in range(1, ntp):
        pl.semaphore_signal(barrier, inc=1, device_id={"tp": lax.rem(t + d, ntp)}, device_id_type=MESH)
    pl.semaphore_wait(barrier, nsp - 1 + ntp - 1)

    def copy(src, dst, send, recv, to):
        return pltpu.make_async_remote_copy(
            src_ref=src, dst_ref=dst, send_sem=send, recv_sem=recv,
            device_id={"sp": to}, device_id_type=MESH)

    side = 2 * z + (1 - y)

    def kv_copy(block, lane, k, p, src=None):
        to = jnp.minimum(s + 2, nsp - 1) if lane == 0 else side
        return copy(kvb.at[block, p] if src is None else src, kvb.at[block, p],
                    kv_s.at[lane, p, k], kv_r.at[p, block], to)

    def qg_copy(block, lane, k, p, src=None):
        to = jnp.maximum(s - 2, 0) if lane == 0 else side
        return copy(qgb.at[block, p] if src is None else src, qgb.at[block, p],
                    qg_s.at[lane, p, k], qg_r.at[p, block], to)

    def st_copy(block, lane, k, src=None):
        to = jnp.maximum(s - 2, 0) if lane == 0 else side
        return copy(stb.at[block] if src is None else src, stb.at[block],
                    st_s.at[lane, k], st_r.at[block], to)

    for p, src in ((0, own_k), (1, own_v)):
        @pl.when(z < nz - 1)
        def _():
            kv_copy(s, 0, 0, p, src).start()

        @pl.when(y == 0)
        def _():
            kv_copy(s, 1, 0, p, src).start()

    @pl.when(z > 0)
    def _():
        qg_copy(s, 0, 0, 0, own_q).start()

    @pl.when(y == 1)
    def _():
        qg_copy(s, 1, 0, 0, own_q).start()

    norm_backward(heads, width, lam, gain, mo, og, lse, own_g, col, row)

    @pl.when(z > 0)
    def _():
        st_copy(s, 0, 0, row).start()
        qg_copy(s, 0, 0, 1, own_g).start()

    @pl.when(y == 1)
    def _():
        st_copy(s, 1, 0, row).start()
        qg_copy(s, 1, 0, 1, own_g).start()

    lane_id = lax.broadcasted_iota(jnp.int32, (1, width), 1)
    low = jnp.where(lane_id < width // 2, 1.0, 0.0).astype(BF16)
    high = jnp.where(lane_id < width // 2, 0.0, 1.0).astype(BF16)

    def split(x):
        return jnp.concatenate([x * low, x * high], axis=0)

    def query_side(k_at, v_at, diagonal):
        def one(h, carry):
            at = pl.ds(pl.multiple_of(h * width, width), width)
            keys = split(k_at[:, at])
            scores = dot_nt(own_q[:, at], keys)
            mixed = dot_nt(own_g[:, at], v_at[:, at])
            stats = col[h]
            x1 = scores[:, :rows] * exp_scale - stats[:, 0:1]
            x2 = scores[:, rows:] * exp_scale - stats[:, 1:2]
            if diagonal:
                seen = (lax.broadcasted_iota(jnp.int32, (rows, rows), 1)
                        <= lax.broadcasted_iota(jnp.int32, (rows, rows), 0))
                x1 = jnp.where(seen, x1, -jnp.inf)
                x2 = jnp.where(seen, x2, -jnp.inf)
            g1 = (jnp.exp2(x1) * (mixed - stats[:, 2:3])).astype(BF16)
            g2 = (jnp.exp2(x2) * (stats[:, 3:4] - mixed)).astype(BF16)
            part_dq = dot_nn(jnp.concatenate([g1, g2], axis=1), keys)
            if diagonal:
                dq_acc[:, at] = part_dq
            else:
                dq_acc[:, at] += part_dq
            return carry
        lax.fori_loop(0, heads, one, 0)

    def key_side(q_at, g_at, row_at, diagonal):
        def one(h, carry):
            at = pl.ds(pl.multiple_of(h * width, width), width)
            queries = split(q_at[:, at])
            grads = g_at[:, at]
            scores = dot_nt(own_k[:, at], queries)
            mixed = dot_nt(own_v[:, at], grads)
            stats = row_at[h]
            x1 = scores[:, :rows] * exp_scale - stats[0:1]
            x2 = scores[:, rows:] * exp_scale - stats[1:2]
            if diagonal:
                seen = (lax.broadcasted_iota(jnp.int32, (rows, rows), 0)
                        <= lax.broadcasted_iota(jnp.int32, (rows, rows), 1))
                x1 = jnp.where(seen, x1, -jnp.inf)
                x2 = jnp.where(seen, x2, -jnp.inf)
            p1 = jnp.exp2(x1)
            p2 = jnp.exp2(x2)
            g1 = (p1 * (mixed - stats[2:3])).astype(BF16)
            g2 = (p2 * (stats[3:4] - mixed)).astype(BF16)
            part_dv = dot_nn((p1 - p2).astype(BF16), grads)
            part_dk = dot_nn(jnp.concatenate([g1, g2], axis=1), queries)
            if diagonal:
                dv_acc[:, at] = part_dv
                dk_acc[:, at] = part_dk
            else:
                dv_acc[:, at] += part_dv
                dk_acc[:, at] += part_dk
            return carry
        lax.fori_loop(0, heads, one, 0)

    def lat_copy(d):
        to = lax.rem(s + d, nsp)
        mine = pl.ds(pl.multiple_of(t * part, part), part)
        return copy(lat.at[mine, pl.ds(pl.multiple_of(to * slab, slab), slab)],
                    latb.at[s, mine, :], la_s.at[d], la_r.at[d], to)

    def own_lat():
        return pltpu.make_async_copy(
            lat.at[pl.ds(pl.multiple_of(t * part, part), part), pl.ds(pl.multiple_of(s * slab, slab), slab)],
            latb.at[s, pl.ds(pl.multiple_of(t * part, part), part), :], own_sem)

    def share_copy(d):
        mine = pl.ds(pl.multiple_of(t * part, part), part)
        return pltpu.make_async_remote_copy(
            src_ref=latb.at[:, mine, :], dst_ref=latb.at[:, mine, :],
            send_sem=lb_s.at[d], recv_sem=lb_r.at[d],
            device_id={"tp": lax.rem(t + d, ntp)}, device_id_type=MESH)

    own_lat().start()
    query_side(own_k, own_v, True)
    key_side(own_q, own_g, row, True)
    for d in range(1, nsp):
        lat_copy(d).start()

    def step(k, carry):
        below, above = z - k, z + k
        has_below, has_above = below >= 0, above < nz
        kb = jnp.maximum(below, 0) * 2 + y
        qb = jnp.minimum(above, nz - 1) * 2 + y

        for p in range(2):
            @pl.when(has_below)
            def _():
                kv_copy(kb, 0, 0, p).wait_recv()
                kv_copy(kb, 1, k, p).start()

            @pl.when(has_below & (z < nz - 1))
            def _():
                kv_copy(kb, 0, k, p).start()

            @pl.when(has_above)
            def _():
                qg_copy(qb, 0, 0, p).wait_recv()
                qg_copy(qb, 1, k, p).start()
                if p == 0:
                    st_copy(qb, 0, 0).wait_recv()
                    st_copy(qb, 1, k).start()

            @pl.when(has_above & (z > 0))
            def _():
                qg_copy(qb, 0, k, p).start()
                if p == 0:
                    st_copy(qb, 0, k).start()

        def turn(c, carry):
            dist = k - c
            other = jnp.where(c == 0, y, 1 - y)
            bz, qz = z - dist, z + dist
            use_kv = (bz >= 0) & (dist < nz) & ((dist > 0) | (y == 1))
            use_qg = (qz < nz) & (dist < nz) & ((dist > 0) | (y == 0))
            kblk = jnp.maximum(bz, 0) * 2 + other
            qblk = jnp.minimum(qz, nz - 1) * 2 + other

            @pl.when(use_kv)
            def _():
                @pl.when(c == 1)
                def _():
                    for p in range(2):
                        kv_copy(kblk, 1, 0, p).wait_recv()
                query_side(kvb.at[kblk, 0], kvb.at[kblk, 1], False)

            @pl.when(use_qg)
            def _():
                @pl.when(c == 1)
                def _():
                    for p in range(2):
                        qg_copy(qblk, 1, 0, p).wait_recv()
                    st_copy(qblk, 1, 0).wait_recv()
                key_side(qgb.at[qblk, 0], qgb.at[qblk, 1], stb.at[qblk], False)
            return carry
        lax.fori_loop(0, 2, turn, 0)
        return carry

    lax.fori_loop(1, nz + 1, step, 0)

    own_dq[...] = (dq_acc[...] * score_scale).astype(BF16)
    half = rows // 2

    def dq_copy(block, lane, idx, p, own=False):
        to = (jnp.minimum(s + 2, nsp - 2 + y), jnp.maximum(s - 2, y), side)[lane]
        at = pl.ds(p * half, half)
        return copy(own_dq.at[at] if own else dqb.at[block, at], dqb.at[block, at],
                    dq_s.at[lane, p, idx], dq_r.at[p, block], to)

    for p in range(2):
        @pl.when(z < nz - 1)
        def _():
            dq_copy(s, 0, z, p, True).start()

        @pl.when(z > 0)
        def _():
            dq_copy(s, 1, z, p, True).start()

        dq_copy(s, 2, z, p, True).start()

    for h in range(heads):
        at = slice(h * width, (h + 1) * width)
        dq_out[:, h, :] = own_dq[:, at]
        dk_out[:, h, :] = (dk_acc[:, at] * score_scale).astype(BF16)
        dv_out[:, h, :] = dv_acc[:, at].astype(BF16)

    own_lat().wait()
    for d in range(1, nsp):
        lat_copy(d).wait_recv()
    for d in range(1, ntp):
        share_copy(d).start()
    for d in range(1, ntp):
        share_copy(d).wait_recv()

    wg_out[...] = dot_tn(latb[s], own_dq[...])

    def add_block(block):
        wg_out[...] += dot_tn(latb[block], dqb[block])

    def gather(k, carry):
        for p in range(2):
            for lane, there, ok, more in (
                (0, z - k, z - k >= 0, z < nz - 1),
                (1, z + k, z + k < nz, z > 0),
            ):
                bz = jnp.clip(there, 0, nz - 1)
                block = bz * 2 + y

                @pl.when(ok)
                def _():
                    dq_copy(block, lane, bz, p).wait_recv()
                    dq_copy(block, 2, bz, p).start()

                @pl.when(ok & more)
                def _():
                    dq_copy(block, lane, bz, p).start()

        def turn(c, carry):
            dist = jnp.where(c < 2, k, k - 1)
            up = lax.rem(c, 2)
            bz = jnp.where(up == 0, z - dist, z + dist)
            ok = (bz >= 0) & (bz < nz) & (dist < nz) & ((dist > 0) | (up == 0))
            other = jnp.where(c < 2, y, 1 - y)
            block = jnp.clip(bz, 0, nz - 1) * 2 + other

            @pl.when(ok)
            def _():
                @pl.when(c >= 2)
                def _():
                    for p in range(2):
                        dq_copy(block, 2, 0, p).wait_recv()
                add_block(block)
            return carry
        lax.fori_loop(0, 4, turn, 0)
        return carry

    lax.fori_loop(1, nz + 1, gather, 0)

    def drain(k, carry):
        below, above = z - k, z + k
        has_below, has_above = below >= 0, above < nz

        for p in range(2):
            @pl.when(has_below & (z < nz - 1))
            def _():
                kv_copy(s, 0, k, p).wait_send()

            @pl.when(has_below & ((k > 0) | (y == 0)))
            def _():
                kv_copy(s, 1, k, p).wait_send()

            @pl.when(has_above & (z > 0))
            def _():
                qg_copy(s, 0, k, p).wait_send()
                if p == 0:
                    st_copy(s, 0, k).wait_send()

            @pl.when(has_above & ((k > 0) | (y == 1)))
            def _():
                qg_copy(s, 1, k, p).wait_send()
                if p == 0:
                    st_copy(s, 1, k).wait_send()

            @pl.when((k <= z) & (z < nz - 1))
            def _():
                dq_copy(s, 0, k, p).wait_send()

            @pl.when((k >= z) & (z > 0))
            def _():
                dq_copy(s, 1, k, p).wait_send()

            dq_copy(s, 2, k, p).wait_send()
        return carry

    lax.fori_loop(0, nz, drain, 0)
    for d in range(1, nsp):
        lat_copy(d).wait_send()
    for d in range(1, ntp):
        share_copy(d).wait_send()


def vmem():
    return pl.BlockSpec(memory_space=pltpu.VMEM)


def body(nsp, ntp, latents, query_heads, key_heads, value_heads, map_outputs, log_sums, out_grad,
         mix_lambda, norm_gain):
    rows, heads, width = query_heads.shape
    flat = (rows, heads * width)
    slab = latents.shape[1] // nsp
    nz = nsp // 2
    dma = pltpu.SemaphoreType.DMA
    dq, dk, dv, wg = pl.pallas_call(
        functools.partial(main_kernel, nsp, ntp, heads, width),
        out_shape=(
            jax.ShapeDtypeStruct(query_heads.shape, BF16),
            jax.ShapeDtypeStruct(query_heads.shape, BF16),
            jax.ShapeDtypeStruct(query_heads.shape, BF16),
            jax.ShapeDtypeStruct((slab, heads * width), F32),
        ),
        in_specs=[pl.BlockSpec(memory_space=pltpu.SMEM)] + [vmem()] * 8,
        out_specs=(vmem(),) * 4,
        scratch_shapes=[
            pltpu.VMEM(flat, BF16),
            pltpu.VMEM((heads, rows, width), F32),
            pltpu.VMEM((heads, 4, rows), F32),
            pltpu.VMEM(flat, BF16),
            pltpu.VMEM((nsp, 2) + flat, BF16),
            pltpu.VMEM((nsp, 2) + flat, BF16),
            pltpu.VMEM((nsp, heads, 4, rows), F32),
            pltpu.VMEM((nsp,) + flat, BF16),
            pltpu.VMEM((nsp, rows, slab), BF16),
            pltpu.VMEM(flat, F32),
            pltpu.VMEM(flat, F32),
            pltpu.VMEM(flat, F32),
            dma((2, 2, nz)), dma((2, 2, nz)), dma((2, nz)), dma((3, 2, nz)),
            dma((2, nsp)), dma((2, nsp)), dma((nsp,)), dma((2, nsp)),
            dma((nsp,)), dma((nsp,)), dma((ntp,)), dma((ntp,)),
            dma,
        ],
        compiler_params=pltpu.CompilerParams(collective_id=0, has_side_effects=True),
        name="main",
    )(
        mix_lambda,
        norm_gain[None, :],
        latents,
        key_heads.reshape(flat),
        value_heads.reshape(flat),
        query_heads.reshape(flat),
        map_outputs,
        out_grad,
        jnp.transpose(log_sums, (1, 0, 2)),
    )
    return dq, dk, dv, wg


def solution(mesh):
    placed = (
        P("sp", None),
        P("sp", "tp", None),
        P("sp", "tp", None),
        P("sp", "tp", None),
        P("sp", None, "tp", None),
        P("sp", "tp", None),
        P("sp", "tp", None),
        P("tp"),
        P(),
    )
    return jax.shard_map(
        functools.partial(body, mesh.shape["sp"], mesh.shape["tp"]),
        mesh=mesh,
        in_specs=placed,
        out_specs=(P("sp", "tp", None), P("sp", "tp", None), P("sp", "tp", None), P("sp", "tp")),
        check_vma=False,
    )
```

profile of v0, /device:TPU:1, one launch (start us, length us, event | category | flops | bytes accessed | tf_op | source)
XLA Modules:
  0.0 115.9 jit_solution(17533509706725338349)
XLA Ops:
  0.6 1.7 %copy.20 = bf16[32,8,4,128]{3,1,2,0:T(8,128)(2,1)} copy(bf16[32,8,4,128]{3,2,1,0:T(4,128)(2,1)} %bitcast.14) | data formatting | bytes 524288
  2.3 1.7 %copy.13 = f32[256,4,2]{2,0,1:T(8,128)} copy(f32[256,4,2]{0,2,1:T(2,128)} %param.14) | data formatting | bytes 16384 | tf_op args[5]
  4.0 1.9 %copy_bitcast_fusion = (bf16[256,512]{1,0:T(8,128)(2,1)}, bf16[256,512]{1,0:T(8,128)(2,1)}) fusion(bf16[32,8,4,128]{3,2,1,0:T(4,128)(2,1)} %bitcast.15, bf16[32,8,4,128]{3,2,1,0:T(4,128)(2,1)} %bitcast.16), kind=kLoop, calls=%fused_computation | loop fusion | bytes 1048576 | tf_op jit(solution)/shard_map/reshape | solution.py:441
  5.9 103.7 %main.1 = (bf16[256,4,128]{2,1,0:T(4,128)(2,1)}, bf16[256,4,128]{2,1,0:T(4,128)(2,1)}, bf16[256,4,128]{2,1,0:T(4,128)(2,1)}, f32[512,512]{1,0:T(8,128)}) custom-call(f32[4]{0:T(128)} %lam.1, f32[1,128]{1,0:T(1,128)} %bitcast.17, bf16[256,4096]{1,0:T(8,128)(2,1)} %lat.1, bf16[256,512]{1,0:T(8,128)(2,1)} %bitcast.13, bf16[256,512]{1,0:T(8,128)(2,1)} %get-tuple-element.5.own_v, ...), custom_call_target="tpu_custom_call" | custom-call | tf_op jit(solution)/shard_map/main/pallas_call | solution.py:405
  109.6 0.0 copy-start
  109.6 1.8 %copy.25 = bf16[256,4,128]{2,1,0:T(4,128)(2,1)} copy(bf16[256,4,128]{2,1,0:T(4,128)(2,1)} %get-tuple-element.10) | data formatting | bytes 524288
  111.4 1.7 %copy.26 = bf16[256,4,128]{2,1,0:T(4,128)(2,1)} copy(bf16[256,4,128]{2,1,0:T(4,128)(2,1)} %get-tuple-element.11) | data formatting | bytes 524288
  113.2 1.7 %copy.27 = bf16[256,4,128]{2,1,0:T(4,128)(2,1)} copy(bf16[256,4,128]{2,1,0:T(4,128)(2,1)} %get-tuple-element.12) | data formatting | bytes 524288
  114.9 0.0 copy-done
  114.9 1.0 copy.28
Async XLA Ops:
  109.6 5.3 %copy-start = (f32[512,512]{1,0:T(8,128)S(1)}, f32[512,512]{1,0:T(8,128)}, u32[]{:S(2)}) copy-start(f32[512,512]{1,0:T(8,128)} %get-tuple-element.13) | copy-start | bytes 3145732
where the time goes:
time: 116 us
  Pallas kernels  104 us (90%)
  local copies, waits for them, and re-layouts  11.6 us (10%)
    pallas_call x1, Pallas kernels, body(): pl.pallas_call(functools.partial(main_kernel, nsp, ntp, heads, width), ou...  104 us
    unnamed x8, local copies, waits for them, and re-layouts  9.7 us

commit v1 on v0

--- a/solution.py
+++ b/solution.py
@@ -446,6 +446,496 @@
     return dq, dk, dv, wg
 
 
+def row_norm_backward(heads, width, lam_ref, gain_ref, mo_ref, og_ref, lse_ref, grad_ref, row_ref):
+    for h in range(heads):
+        first = mo_ref[:, 0, h, :].astype(F32)
+        second = mo_ref[:, 1, h, :].astype(F32)
+        lam = lam_ref[h]
+        combined = first - lam * second
+        inverse = lax.rsqrt(jnp.mean(combined * combined, axis=-1, keepdims=True) + EPSILON)
+        weighted = gain_ref[...] * og_ref[:, h, :].astype(F32)
+        grad = (
+            inverse * weighted
+            - inverse**3 * combined * jnp.mean(combined * weighted, axis=-1, keepdims=True)
+        ).astype(BF16)
+        grad_ref[:, h * width : (h + 1) * width] = grad
+        wide = grad.astype(F32)
+        lse = lse_ref[h] * LOG2E
+        log_lam = jnp.log(jnp.full((1, 1), lam, F32)) * LOG2E
+        lane = lax.broadcasted_iota(jnp.int32, wide.shape, 1)
+        stats = jnp.where(lane == 0, lse[:, 0:1], lse[:, 1:2] - log_lam)
+        stats = jnp.where(lane == 2, jnp.sum(wide * first, axis=-1, keepdims=True), stats)
+        stats = jnp.where(lane == 3, jnp.sum(wide * second, axis=-1, keepdims=True), stats)
+        row_ref[h] = jnp.transpose(stats)[0:4]
+
+
+def hub_kernel(nsp, ntp, heads, width, lam, gain, lat, own_k, own_v, own_q, mo, og, lse,
+               dq_out, dk_out, dv_out, wg_out,
+               own_g, row, blk, stb, dq_acc, dk_acc, dv_acc, db, out_b, in_b, in_a, kt, kin, kst, kret, latb,
+               f_s, z_s, b_r, st_r, d_s, d_r, ob_s, ib_r, ia_r, kt_s, kin_r, kst_s, kret_r,
+               la_s, la_r, lb_s, lb_r, own_sem):
+    nz = nsp // 2
+    low, high, top = nz // 2 - 1, nz // 2, nz - 1
+    s = lax.axis_index("sp")
+    t = lax.axis_index("tp")
+    z, y = s // 2, lax.rem(s, 2)
+    rows = own_k.shape[0]
+    span = 2 * rows
+    pair = heads // 2
+    lanes = pair * width
+    part = rows // ntp
+    slab = lat.shape[1] // nsp
+    score_scale = (width // 2) ** (-0.5)
+    exp_scale = score_scale * LOG2E
+    partner = 2 * z + 1 - y
+    Q, K, V, G, ST = range(5)
+
+    barrier = pltpu.get_barrier_semaphore()
+    for d in range(1, nsp):
+        pl.semaphore_signal(barrier, inc=1, device_id={"sp": lax.rem(s + d, nsp)}, device_id_type=MESH)
+    for d in range(1, ntp):
+        pl.semaphore_signal(barrier, inc=1, device_id={"tp": lax.rem(t + d, ntp)}, device_id_type=MESH)
+    pl.semaphore_wait(barrier, nsp - 1 + ntp - 1)
+
+    def copy(src, dst, send, recv, to):
+        return pltpu.make_async_remote_copy(
+            src_ref=src, dst_ref=dst, send_sem=send, recv_sem=recv,
+            device_id={"sp": to}, device_id_type=MESH)
+
+    def at_level(level):
+        return 2 * level + y
+
+    def lane_of(p):
+        return pl.ds(pl.multiple_of(p * lanes, lanes), lanes)
+
+    def half_of(p):
+        return pl.ds(pl.multiple_of(p * rows, rows), rows)
+
+    owned = (own_q, own_k, own_v, own_g)
+
+    def source(a, p):
+        if a == ST:
+            return row.at[pl.ds(p * pair, pair)]
+        return owned[a].at[:, lane_of(p)]
+
+    def landing(a, level, half):
+        return stb.at[level, half] if a == ST else blk.at[a, level, half_of(half), :]
+
+    def landed(a, level, half):
+        return st_r.at[level, half] if a == ST else b_r.at[a, level, half]
+
+    def swap(a):
+        return copy(source(a, 1 - y), landing(a, z, y), f_s.at[a], landed(a, z, y), partner)
+
+    def arrive(a, level, half):
+        copy(landing(a, level, half), landing(a, level, half), f_s.at[a], landed(a, level, half), partner).wait_recv()
+
+    def pass_on(a, own, lane):
+        half = y if own else 1 - y
+        to = low if lane == 0 else high
+        return copy(source(a, y) if own else landing(a, z, half), landing(a, z, half),
+                    z_s.at[lane, a, 0 if own else 1], landed(a, z, half), at_level(to))
+
+    def passes(action, arrays, own):
+        for a in arrays:
+            if a in (K, V):
+                @pl.when(z < low)
+                def _():
+                    action(pass_on(a, own, 0))
+            else:
+                @pl.when(z >= high)
+                def _():
+                    action(pass_on(a, own, 0))
+
+                @pl.when(z > high)
+                def _():
+                    action(pass_on(a, own, 1))
+
+    def start(c):
+        c.start()
+
+    swap(Q).start()
+    passes(start, (Q, K, V), True)
+    swap(K).start()
+    swap(V).start()
+
+    row_norm_backward(heads, width, lam, gain, mo, og, lse, own_g, row)
+
+    swap(G).start()
+    swap(ST).start()
+    passes(start, (ST, G), True)
+
+    for a in (Q, K, V, G):
+        blk[a, z, half_of(y), :] = owned[a][:, lane_of(y)]
+    stb[z, y] = row[pl.ds(y * pair, pair)]
+    dq_acc[...] = jnp.zeros_like(dq_acc)
+    dk_acc[...] = jnp.zeros_like(dk_acc)
+    dv_acc[...] = jnp.zeros_like(dv_acc)
+
+    for a in (Q, K, V, ST, G):
+        arrive(a, z, 1 - y)
+        passes(start, (a,), False)
+
+    lane_id = lax.broadcasted_iota(jnp.int32, (1, width), 1)
+    first_map = jnp.where(lane_id < width // 2, 1.0, 0.0).astype(BF16)
+    second_map = jnp.where(lane_id < width // 2, 0.0, 1.0).astype(BF16)
+
+    def split(x):
+        return jnp.concatenate([x * first_map, x * second_map], axis=0)
+
+    def visit(qz, kz, slot, diagonal):
+        def one(h, carry):
+            at = pl.ds(pl.multiple_of(h * width, width), width)
+            for a in range(2):
+                start_row = a * rows if diagonal else 0
+                kr = pl.ds(a * rows, rows)
+                qr = pl.ds(start_row, span - start_row)
+                count = span - start_row
+                keys = split(blk[K, kz, kr, at])
+                queries = split(blk[Q, qz, qr, at])
+                grads = blk[G, qz, qr, at]
+                scores = dot_nt(blk[K, kz, kr, at], queries)
+                mixed = dot_nt(blk[V, kz, kr, at], grads)
+                stats = jnp.concatenate([stb[qz, p, h] for p in range(start_row // rows, 2)], axis=1)
+                x1 = scores[:, :count] * exp_scale - stats[0:1]
+                x2 = scores[:, count:] * exp_scale - stats[1:2]
+                if diagonal:
+                    seen = (lax.broadcasted_iota(jnp.int32, (rows, count), 0)
+                            <= lax.broadcasted_iota(jnp.int32, (rows, count), 1))
+                    x1 = jnp.where(seen, x1, -jnp.inf)
+                    x2 = jnp.where(seen, x2, -jnp.inf)
+                p1 = jnp.exp2(x1)
+                p2 = jnp.exp2(x2)
+                g1 = (p1 * (mixed - stats[2:3])).astype(BF16)
+                g2 = (p2 * (stats[3:4] - mixed)).astype(BF16)
+                dv_acc[slot, kr, at] += dot_nn((p1 - p2).astype(BF16), grads)
+                dk_acc[slot, kr, at] += dot_nn(jnp.concatenate([g1, g2], axis=1), queries)
+                dq_acc[qz, h, :, qr] += dot_tn(keys, jnp.concatenate([g1, g2], axis=0))
+            return carry
+        lax.fori_loop(0, pair, one, 0)
+
+    def dq_value(level):
+        return jnp.concatenate([jnp.transpose(dq_acc[level, h]) for h in range(pair)], axis=1) * score_scale
+
+    def grad_copy(level, lane):
+        if lane == 0:
+            to = partner
+        elif lane == 1:
+            to = at_level(jnp.where(z == low, 0, jnp.where(z == high, top, low)))
+        else:
+            to = at_level(high)
+        return copy(db.at[level, y], db.at[level, y], d_s.at[level, lane], d_r.at[level, y], to)
+
+    def grad_lanes(level):
+        chained = (z == high) | ((z == low) if level >= low else (z < low))
+        if level > low:
+            return ((0, None), (1, chained))
+        return ((0, None), (1, chained), (2, z == level))
+
+    def grad_each(level, action):
+        for lane, ok in reversed(grad_lanes(level)):
+            if ok is None:
+                action(grad_copy(level, lane))
+            else:
+                @pl.when(ok)
+                def _():
+                    action(grad_copy(level, lane))
+
+    def grad_arrive(level, p):
+        copy(db.at[level, p], db.at[level, p], d_s.at[level, 0], d_r.at[level, p], partner).wait_recv()
+
+    def part_copy(i):
+        return copy(out_b.at[i], in_b.at[i], ob_s.at[i], ib_r.at[i], at_level(jnp.where(z == low, high, low)))
+
+    def top_copy():
+        return copy(out_b.at[0], in_a, ob_s.at[0], ia_r, at_level(high))
+
+    def key_copy(i):
+        return copy(kt.at[i], kin.at[i], kt_s.at[i], kin_r.at[i], at_level(0))
+
+    def return_copy(i):
+        return copy(kst.at[i], kret.at[i, y], kst_s.at[i], kret_r.at[i], partner)
+
+    def lat_copy(d):
+        to = lax.rem(s + d, nsp)
+        mine = pl.ds(pl.multiple_of(t * part, part), part)
+        return copy(lat.at[mine, pl.ds(pl.multiple_of(to * slab, slab), slab)],
+                    latb.at[s, mine, :], la_s.at[d], la_r.at[s], to)
+
+    def own_lat():
+        return pltpu.make_async_copy(
+            lat.at[:, pl.ds(pl.multiple_of(s * slab, slab), slab)], latb.at[s], own_sem)
+
+    def share_copy(b, d):
+        mine = pl.ds(pl.multiple_of(t * part, part), part)
+        return pltpu.make_async_remote_copy(
+            src_ref=latb.at[b, mine, :], dst_ref=latb.at[b, mine, :],
+            send_sem=lb_s.at[b, d], recv_sem=lb_r.at[b, d],
+            device_id={"tp": lax.rem(t + d, ntp)}, device_id_type=MESH)
+
+    def lat_send(descending):
+        for d in range(1, nsp):
+            to = lax.rem(s + d, nsp)
+            down = (z >= high) & (to // 2 < high)
+
+            @pl.when(down if descending else jnp.logical_not(down))
+            def _():
+                lat_copy(d).start()
+
+    def lat_share(descending):
+        def step(d, carry):
+            b = lax.rem(s + d, nsp)
+            down = (z < high) & (b // 2 >= high)
+
+            @pl.when(down if descending else jnp.logical_not(down))
+            def _():
+                mine = pl.ds(pl.multiple_of(t * part, part), part)
+                copy(latb.at[b, mine, :], latb.at[b, mine, :], la_s.at[1], la_r.at[b], partner).wait_recv()
+                for e in range(1, ntp):
+                    share_copy(b, e).start()
+            return carry
+        lax.fori_loop(1, nsp, step, 0)
+
+    own_lat().start()
+    visit(z, z, 0, True)
+
+    @pl.when(z < low)
+    def _():
+        db[0, y] = dq_value(0).astype(BF16)
+        grad_each(0, start)
+
+    @pl.when(z >= high)
+    def _():
+        out_b[0] = dq_value(z).astype(BF16)
+
+    @pl.when(z == high)
+    def _():
+        part_copy(0).start()
+
+    @pl.when(z > high)
+    def _():
+        top_copy().start()
+
+    lat_send(False)
+
+    @pl.when(z == low)
+    def _():
+        def step(i, carry):
+            qz = jnp.where(i == 0, low, high + (i - 1) // 2)
+            kz = jnp.where(i == 0, 0, lax.rem(i - 1, 2))
+
+            @pl.when(i == 0)
+            def _():
+                for half in range(2):
+                    arrive(K, 0, half)
+                    arrive(V, 0, half)
+
+            @pl.when((i > 0) & (kz == 0))
+            def _():
+                for a in (Q, ST, G):
+                    for half in range(2):
+                        arrive(a, qz, half)
+
+            visit(qz, kz, 1 - kz, False)
+
+            @pl.when(i == 0)
+            def _():
+                db[low, y] = dq_value(low).astype(BF16)
+                grad_each(low, start)
+
+            @pl.when((i > 0) & (kz == 1))
+            def _():
+                out_b[qz - high] = dq_value(qz).astype(BF16)
+                part_copy(qz - high).start()
+
+            @pl.when((qz == top) & (kz == 0))
+            def _():
+                kt[0] = (dk_acc[1] * score_scale).astype(BF16)
+                kt[1] = dv_acc[1].astype(BF16)
+                key_copy(0).start()
+                key_copy(1).start()
+            return carry
+        lax.fori_loop(0, 5, step, 0)
+
+    @pl.when(z == high)
+    def _():
+        for a in (Q, ST, G):
+            for half in range(2):
+                arrive(a, top, half)
+        visit(top, high, 0, False)
+        top_copy().wait_recv()
+        out_b[1] = (dq_value(top) + in_a[...].astype(F32)).astype(BF16)
+        part_copy(1).start()
+
+    lat_send(True)
+
+    def finish_keys(extra):
+        for i, acc, scale in ((0, dk_acc, score_scale), (1, dv_acc, 1.0)):
+            other = acc[0, half_of(1 - y), :] * scale
+            mine = acc[0, half_of(y), :] * scale
+            if extra:
+                other += kin[i, half_of(1 - y), :].astype(F32)
+                mine += kin[i, half_of(y), :].astype(F32)
+            kst[i] = other.astype(BF16)
+            return_copy(i).start()
+            kret[i, y] = mine.astype(BF16)
+
+    @pl.when(z >= low)
+    def _():
+        finish_keys(False)
+
+    for level in (0, low):
+        @pl.when(z != level)
+        def _():
+            grad_arrive(level, y)
+            grad_each(level, start)
+
+    lat_share(False)
+
+    @pl.when(z < low)
+    def _():
+        for i in range(2):
+            key_copy(i).wait_recv()
+        finish_keys(True)
+
+    for level in (high, top):
+        i = level - high
+
+        @pl.when((z == low) | (z == high))
+        def _():
+            part_copy(i).wait_recv()
+            total = dq_value(level) + in_b[i].astype(F32)
+            if level == top:
+                above = in_a[...].astype(F32)
+                total = total + jnp.where(z == high, above, jnp.zeros_like(above))
+            db[level, y] = total.astype(BF16)
+
+        @pl.when((z != low) & (z != high))
+        def _():
+            grad_arrive(level, y)
+        grad_each(level, start)
+
+    lat_share(True)
+    own_lat().wait()
+
+    for level in range(nz):
+        grad_arrive(level, 1 - y)
+        for half in range(2):
+            b = 2 * level + half
+
+            @pl.when(s != b)
+            def _():
+                for e in range(1, ntp):
+                    share_copy(b, e).wait_recv()
+        feed = latb[2 * level : 2 * level + 2].reshape(span, slab)
+        for p in range(2):
+            at = slice(p * lanes, (p + 1) * lanes)
+            term = dot_tn(feed, db[level, p])
+            if level == 0:
+                wg_out[:, at] = term
+            else:
+                wg_out[:, at] += term
+
+    for i in range(2):
+        return_copy(i).wait_recv()
+        out = dk_out if i == 0 else dv_out
+        for p in range(2):
+            for h in range(pair):
+                out[:, p * pair + h, :] = kret[i, p, :, h * width : (h + 1) * width]
+    for p in range(2):
+        for h in range(pair):
+            dq_out[:, p * pair + h, :] = db[z, p, half_of(y), h * width : (h + 1) * width]
+
+    def sent(c):
+        c.wait_send()
+
+    for a in range(5):
+        sent(swap(a))
+    for own in (True, False):
+        passes(sent, (Q, K, V, ST, G), own)
+    for level in range(nz):
+        grad_each(level, sent)
+    for i in range(2):
+        sent(return_copy(i))
+
+        @pl.when((z == low) | (z == high))
+        def _():
+            sent(part_copy(i))
+
+        @pl.when(z == low)
+        def _():
+            sent(key_copy(i))
+
+    @pl.when(z > high)
+    def _():
+        sent(top_copy())
+    for d in range(1, nsp):
+        sent(lat_copy(d))
+
+    def drain(d, carry):
+        for e in range(1, ntp):
+            sent(share_copy(lax.rem(s + d, nsp), e))
+        return carry
+    lax.fori_loop(1, nsp, drain, 0)
+
+
+def hub_body(nsp, ntp, latents, query_heads, key_heads, value_heads, map_outputs, log_sums, out_grad,
+             mix_lambda, norm_gain):
+    rows, heads, width = query_heads.shape
+    flat = (rows, heads * width)
+    slab = latents.shape[1] // nsp
+    nz = nsp // 2
+    pair = heads // 2
+    block = (2 * rows, pair * width)
+    half = (rows, pair * width)
+    dma = pltpu.SemaphoreType.DMA
+    return pl.pallas_call(
+        functools.partial(hub_kernel, nsp, ntp, heads, width),
+        out_shape=(
+            jax.ShapeDtypeStruct(query_heads.shape, BF16),
+            jax.ShapeDtypeStruct(query_heads.shape, BF16),
+            jax.ShapeDtypeStruct(query_heads.shape, BF16),
+            jax.ShapeDtypeStruct((slab, heads * width), F32),
+        ),
+        in_specs=[pl.BlockSpec(memory_space=pltpu.SMEM)] + [vmem()] * 8,
+        out_specs=(vmem(),) * 4,
+        scratch_shapes=[
+            pltpu.VMEM(flat, BF16),
+            pltpu.VMEM((heads, 4, rows), F32),
+            pltpu.VMEM((4, nz) + block, BF16),
+            pltpu.VMEM((nz, 2, pair, 4, rows), F32),
+            pltpu.VMEM((nz, pair, width, 2 * rows), F32),
+            pltpu.VMEM((2,) + block, F32),
+            pltpu.VMEM((2,) + block, F32),
+            pltpu.VMEM((nz, 2) + block, BF16),
+            pltpu.VMEM((2,) + block, BF16),
+            pltpu.VMEM((2,) + block, BF16),
+            pltpu.VMEM(block, BF16),
+            pltpu.VMEM((2,) + block, BF16),
+            pltpu.VMEM((2,) + block, BF16),
+            pltpu.VMEM((2,) + half, BF16),
+            pltpu.VMEM((2, 2) + half, BF16),
+            pltpu.VMEM((nsp, rows, slab), BF16),
+            dma((5,)), dma((2, 5, 2)), dma((4, nz, 2)), dma((nz, 2)), dma((nz, 3)), dma((nz, 2)),
+            dma((2,)), dma((2,)), dma, dma((2,)), dma((2,)), dma((2,)), dma((2,)),
+            dma((nsp,)), dma((nsp,)), dma((nsp, ntp)), dma((nsp, ntp)),
+            dma,
+        ],
+        compiler_params=pltpu.CompilerParams(collective_id=0, has_side_effects=True),
+        name="hub",
+    )(
+        mix_lambda,
+        norm_gain[None, :],
+        latents,
+        key_heads.reshape(flat),
+        value_heads.reshape(flat),
+        query_heads.reshape(flat),
+        map_outputs,
+        out_grad,
+        jnp.transpose(log_sums, (1, 0, 2)),
+    )
+
+
 def solution(mesh):
     placed = (
         P("sp", None),
@@ -458,8 +948,14 @@
         P("tp"),
         P(),
     )
+    nsp, ntp = mesh.shape["sp"], mesh.shape["tp"]
+
+    def chosen(*args):
+        heads = args[1].shape[1]
+        return (hub_body if nsp == 8 and heads % 2 == 0 else body)(nsp, ntp, *args)
+
     return jax.shard_map(
-        functools.partial(body, mesh.shape["sp"], mesh.shape["tp"]),
+        chosen,
         mesh=mesh,
         in_specs=placed,
         out_specs=(P("sp", "tp", None), P("sp", "tp", None), P("sp", "tp", None), P("sp", "tp")),

time: 116 us -> 101 us (0.87)
  the two profiles are of different devices: /device:TPU:1 before, /device:TPU:0 now
where the time goes in v1:
time: 101 us; the launch traced here: 100 us
  Pallas kernels  88 us (87%)
  local copies, waits for them, and re-layouts  11.6 us (11%)
    pallas_call x1, Pallas kernels, hub_body(): pl.pallas_call(functools.partial(hub_kernel, nsp, ntp, heads, width), out...  88 us
    unnamed x8, local copies, waits for them, and re-layouts  9.7 us

profile of v1, /device:TPU:0, one launch (start us, length us, event | category | flops | bytes accessed | tf_op | source)
XLA Modules:
  0.0 100.2 jit_solution(4973878991067109572)
XLA Ops:
  0.6 1.7 %copy.20 = bf16[32,8,4,128]{3,1,2,0:T(8,128)(2,1)} copy(bf16[32,8,4,128]{3,2,1,0:T(4,128)(2,1)} %bitcast.14) | data formatting | bytes 524288
  2.3 1.7 %copy.13 = f32[256,4,2]{2,0,1:T(8,128)} copy(f32[256,4,2]{0,2,1:T(2,128)} %param.14) | data formatting | bytes 16384 | tf_op args[5]
  4.0 1.9 %copy_bitcast_fusion = (bf16[256,512]{1,0:T(8,128)(2,1)}, bf16[256,512]{1,0:T(8,128)(2,1)}) fusion(bf16[32,8,4,128]{3,2,1,0:T(4,128)(2,1)} %bitcast.15, bf16[32,8,4,128]{3,2,1,0:T(4,128)(2,1)} %bitcast.16), kind=kLoop, calls=%fused_computation | loop fusion | bytes 1048576 | tf_op jit(solution)/shard_map/reshape | solution.py:932
  5.9 88.0 %hub.1 = (bf16[256,4,128]{2,1,0:T(4,128)(2,1)}, bf16[256,4,128]{2,1,0:T(4,128)(2,1)}, bf16[256,4,128]{2,1,0:T(4,128)(2,1)}, f32[512,512]{1,0:T(8,128)}) custom-call(f32[4]{0:T(128)} %lam.1, f32[1,128]{1,0:T(1,128)} %bitcast.17, bf16[256,4096]{1,0:T(8,128)(2,1)} %lat.1, bf16[256,512]{1,0:T(8,128)(2,1)} %bitcast.13, bf16[256,512]{1,0:T(8,128)(2,1)} %get-tuple-element.5.own_v, ...), custom_call_target="tpu_custom_call" | custom-call | tf_op jit(solution)/shard_map/hub/pallas_call | solution.py:892
  93.9 0.0 copy-start
  93.9 1.8 %copy.25 = bf16[256,4,128]{2,1,0:T(4,128)(2,1)} copy(bf16[256,4,128]{2,1,0:T(4,128)(2,1)} %get-tuple-element.10) | data formatting | bytes 524288
  95.8 1.7 %copy.26 = bf16[256,4,128]{2,1,0:T(4,128)(2,1)} copy(bf16[256,4,128]{2,1,0:T(4,128)(2,1)} %get-tuple-element.11) | data formatting | bytes 524288
  97.5 1.7 %copy.27 = bf16[256,4,128]{2,1,0:T(4,128)(2,1)} copy(bf16[256,4,128]{2,1,0:T(4,128)(2,1)} %get-tuple-element.12) | data formatting | bytes 524288
  99.3 0.0 copy-done
  99.3 1.0 copy.28
Async XLA Ops:
  93.9 5.3 %copy-start = (f32[512,512]{1,0:T(8,128)S(1)}, f32[512,512]{1,0:T(8,128)}, u32[]{:S(2)}) copy-start(f32[512,512]{1,0:T(8,128)} %get-tuple-element.13) | copy-start | bytes 3145732

commit v2 on v1

--- a/solution.py
+++ b/solution.py
@@ -460,19 +460,19 @@
         ).astype(BF16)
         grad_ref[:, h * width : (h + 1) * width] = grad
         wide = grad.astype(F32)
-        lse = lse_ref[h] * LOG2E
         log_lam = jnp.log(jnp.full((1, 1), lam, F32)) * LOG2E
+        row_ref[h, 0:1] = lse_ref[h, 0:1] * LOG2E
+        row_ref[h, 1:2] = lse_ref[h, 1:2] * LOG2E - log_lam
         lane = lax.broadcasted_iota(jnp.int32, wide.shape, 1)
-        stats = jnp.where(lane == 0, lse[:, 0:1], lse[:, 1:2] - log_lam)
-        stats = jnp.where(lane == 2, jnp.sum(wide * first, axis=-1, keepdims=True), stats)
-        stats = jnp.where(lane == 3, jnp.sum(wide * second, axis=-1, keepdims=True), stats)
-        row_ref[h] = jnp.transpose(stats)[0:4]
+        terms = jnp.where(lane == 0, jnp.sum(wide * first, axis=-1, keepdims=True),
+                          jnp.sum(wide * second, axis=-1, keepdims=True))
+        row_ref[h, 2:4] = jnp.transpose(terms)[0:2]
 
 
 def hub_kernel(nsp, ntp, heads, width, lam, gain, lat, own_k, own_v, own_q, mo, og, lse,
                dq_out, dk_out, dv_out, wg_out,
                own_g, row, blk, stb, dq_acc, dk_acc, dv_acc, db, out_b, in_b, in_a, kt, kin, kst, kret, latb,
-               f_s, z_s, b_r, st_r, d_s, d_r, ob_s, ib_r, ia_r, kt_s, kin_r, kst_s, kret_r,
+               f_s, z_s, r_s, b_r, st_r, d_s, d_r, ob_s, ib_r, ia_r, kt_s, kin_r, tot_s, kst_s, kret_r,
                la_s, la_r, lb_s, lb_r, own_sem):
     nz = nsp // 2
     low, high, top = nz // 2 - 1, nz // 2, nz - 1
@@ -530,34 +530,83 @@
     def arrive(a, level, half):
         copy(landing(a, level, half), landing(a, level, half), f_s.at[a], landed(a, level, half), partner).wait_recv()
 
-    def pass_on(a, own, lane):
+    def pass_on(a, own):
         half = y if own else 1 - y
-        to = low if lane == 0 else high
         return copy(source(a, y) if own else landing(a, z, half), landing(a, z, half),
-                    z_s.at[lane, a, 0 if own else 1], landed(a, z, half), at_level(to))
+                    z_s.at[a, 0 if own else 1], landed(a, z, half), at_level(jnp.where(z > high, high, low)))
 
     def passes(action, arrays, own):
         for a in arrays:
             if a in (K, V):
                 @pl.when(z < low)
                 def _():
-                    action(pass_on(a, own, 0))
+                    action(pass_on(a, own))
             else:
                 @pl.when(z >= high)
                 def _():
-                    action(pass_on(a, own, 0))
-
-                @pl.when(z > high)
-                def _():
-                    action(pass_on(a, own, 1))
+                    action(pass_on(a, own))
+
+    def relay(a, half):
+        return copy(landing(a, top, half), landing(a, top, half), r_s.at[a, half], landed(a, top, half), at_level(low))
+
+    def relays(arrays, half):
+        @pl.when(z == high)
+        def _():
+            for a in arrays:
+                arrive(a, top, half)
+                relay(a, half).start()
 
     def start(c):
         c.start()
+
+    def lat_copy(d):
+        to = lax.rem(s + d, nsp)
+        mine = pl.ds(pl.multiple_of(t * part, part), part)
+        return copy(lat.at[mine, pl.ds(pl.multiple_of(to * slab, slab), slab)],
+                    latb.at[s, mine, :], la_s.at[d], la_r.at[s], to)
+
+    def own_lat():
+        return pltpu.make_async_copy(
+            lat.at[:, pl.ds(pl.multiple_of(s * slab, slab), slab)], latb.at[s], own_sem)
+
+    def share_copy(b, d):
+        mine = pl.ds(pl.multiple_of(t * part, part), part)
+        return pltpu.make_async_remote_copy(
+            src_ref=latb.at[b, mine, :], dst_ref=latb.at[b, mine, :],
+            send_sem=lb_s.at[b, d], recv_sem=lb_r.at[b, d],
+            device_id={"tp": lax.rem(t + d, ntp)}, device_id_type=MESH)
+
+    def group_of(src, dst, group):
+        sz, dz = src // 2, dst // 2
+        first = (lax.rem(src, 2) == lax.rem(dst, 2)) & ((dz > sz) | ((dz < sz) & (sz < high)))
+        last = (sz >= high) & (dz < high)
+        return first if group == 0 else last if group == 2 else jnp.logical_not(first | last)
+
+    def lat_send(group):
+        for d in range(1, nsp):
+            @pl.when(group_of(s, lax.rem(s + d, nsp), group))
+            def _():
+                lat_copy(d).start()
+
+    def lat_share(group):
+        def step(d, carry):
+            b = lax.rem(s + d, nsp)
+
+            @pl.when(group_of(b, s, group))
+            def _():
+                mine = pl.ds(pl.multiple_of(t * part, part), part)
+                copy(latb.at[b, mine, :], latb.at[b, mine, :], la_s.at[1], la_r.at[b], partner).wait_recv()
+                for e in range(1, ntp):
+                    share_copy(b, e).start()
+            return carry
+        lax.fori_loop(1, nsp, step, 0)
 
     swap(Q).start()
     passes(start, (Q, K, V), True)
     swap(K).start()
     swap(V).start()
+    lat_send(0)
+    own_lat().start()
 
     row_norm_backward(heads, width, lam, gain, mo, og, lse, own_g, row)
 
@@ -575,6 +624,11 @@
     for a in (Q, K, V, ST, G):
         arrive(a, z, 1 - y)
         passes(start, (a,), False)
+        if a == Q:
+            relays((Q,), y)
+        if a == G:
+            relays((Q,), 1 - y)
+            relays((ST, G), y)
 
     lane_id = lax.broadcasted_iota(jnp.int32, (1, width), 1)
     first_map = jnp.where(lane_id < width // 2, 1.0, 0.0).astype(BF16)
@@ -651,58 +705,23 @@
         return copy(out_b.at[0], in_a, ob_s.at[0], ia_r, at_level(high))
 
     def key_copy(i):
-        return copy(kt.at[i], kin.at[i], kt_s.at[i], kin_r.at[i], at_level(0))
+        return copy(kt.at[i], kin.at[i], kt_s.at[i], kin_r.at[i], at_level(low))
+
+    def total_copy(i, half):
+        return copy(kt.at[i, half_of(half), :], kret.at[i, y], tot_s.at[i, half], kret_r.at[i, y], half)
 
     def return_copy(i):
-        return copy(kst.at[i], kret.at[i, y], kst_s.at[i], kret_r.at[i], partner)
-
-    def lat_copy(d):
-        to = lax.rem(s + d, nsp)
-        mine = pl.ds(pl.multiple_of(t * part, part), part)
-        return copy(lat.at[mine, pl.ds(pl.multiple_of(to * slab, slab), slab)],
-                    latb.at[s, mine, :], la_s.at[d], la_r.at[s], to)
-
-    def own_lat():
-        return pltpu.make_async_copy(
-            lat.at[:, pl.ds(pl.multiple_of(s * slab, slab), slab)], latb.at[s], own_sem)
-
-    def share_copy(b, d):
-        mine = pl.ds(pl.multiple_of(t * part, part), part)
-        return pltpu.make_async_remote_copy(
-            src_ref=latb.at[b, mine, :], dst_ref=latb.at[b, mine, :],
-            send_sem=lb_s.at[b, d], recv_sem=lb_r.at[b, d],
-            device_id={"tp": lax.rem(t + d, ntp)}, device_id_type=MESH)
-
-    def lat_send(descending):
-        for d in range(1, nsp):
-            to = lax.rem(s + d, nsp)
-            down = (z >= high) & (to // 2 < high)
-
-            @pl.when(down if descending else jnp.logical_not(down))
-            def _():
-                lat_copy(d).start()
-
-    def lat_share(descending):
-        def step(d, carry):
-            b = lax.rem(s + d, nsp)
-            down = (z < high) & (b // 2 >= high)
-
-            @pl.when(down if descending else jnp.logical_not(down))
-            def _():
-                mine = pl.ds(pl.multiple_of(t * part, part), part)
-                copy(latb.at[b, mine, :], latb.at[b, mine, :], la_s.at[1], la_r.at[b], partner).wait_recv()
-                for e in range(1, ntp):
-                    share_copy(b, e).start()
-            return carry
-        lax.fori_loop(1, nsp, step, 0)
-
-    own_lat().start()
+        return copy(kst.at[i], kret.at[i, y], kst_s.at[i], kret_r.at[i, y], partner)
+
     visit(z, z, 0, True)
 
     @pl.when(z < low)
     def _():
         db[0, y] = dq_value(0).astype(BF16)
         grad_each(0, start)
+        for i in range(2):
+            kt[i] = (dv_acc[0] if i else dk_acc[0] * score_scale).astype(BF16)
+            key_copy(i).start()
 
     @pl.when(z >= high)
     def _():
@@ -716,7 +735,8 @@
     def _():
         top_copy().start()
 
-    lat_send(False)
+    lat_send(1)
+    lat_share(0)
 
     @pl.when(z == low)
     def _():
@@ -750,39 +770,32 @@
 
             @pl.when((qz == top) & (kz == 0))
             def _():
-                kt[0] = (dk_acc[1] * score_scale).astype(BF16)
-                kt[1] = dv_acc[1].astype(BF16)
-                key_copy(0).start()
-                key_copy(1).start()
+                for j in range(2):
+                    key_copy(j).wait_recv()
+                    acc = dv_acc[1] if j else dk_acc[1] * score_scale
+                    kt[j] = (acc + kin[j].astype(F32)).astype(BF16)
+                    for half in range(2):
+                        total_copy(j, half).start()
             return carry
         lax.fori_loop(0, 5, step, 0)
 
+    relays((ST, G), 1 - y)
+
     @pl.when(z == high)
     def _():
-        for a in (Q, ST, G):
-            for half in range(2):
-                arrive(a, top, half)
         visit(top, high, 0, False)
         top_copy().wait_recv()
         out_b[1] = (dq_value(top) + in_a[...].astype(F32)).astype(BF16)
         part_copy(1).start()
 
-    lat_send(True)
-
-    def finish_keys(extra):
+    lat_send(2)
+
+    @pl.when(z >= low)
+    def _():
         for i, acc, scale in ((0, dk_acc, score_scale), (1, dv_acc, 1.0)):
-            other = acc[0, half_of(1 - y), :] * scale
-            mine = acc[0, half_of(y), :] * scale
-            if extra:
-                other += kin[i, half_of(1 - y), :].astype(F32)
-                mine += kin[i, half_of(y), :].astype(F32)
-            kst[i] = other.astype(BF16)
+            kst[i] = (acc[0, half_of(1 - y), :] * scale).astype(BF16)
             return_copy(i).start()
-            kret[i, y] = mine.astype(BF16)
-
-    @pl.when(z >= low)
-    def _():
-        finish_keys(False)
+            kret[i, y] = (acc[0, half_of(y), :] * scale).astype(BF16)
 
     for level in (0, low):
         @pl.when(z != level)
@@ -790,13 +803,7 @@
             grad_arrive(level, y)
             grad_each(level, start)
 
-    lat_share(False)
-
-    @pl.when(z < low)
-    def _():
-        for i in range(2):
-            key_copy(i).wait_recv()
-        finish_keys(True)
+    lat_share(1)
 
     for level in (high, top):
         i = level - high
@@ -815,7 +822,7 @@
             grad_arrive(level, y)
         grad_each(level, start)
 
-    lat_share(True)
+    lat_share(2)
     own_lat().wait()
 
     for level in range(nz):
@@ -837,14 +844,16 @@
                 wg_out[:, at] += term
 
     for i in range(2):
-        return_copy(i).wait_recv()
+        copy(kst.at[i], kret.at[i, 1 - y], kst_s.at[i], kret_r.at[i, 1 - y], partner).wait_recv()
+
+        @pl.when(z < low)
+        def _():
+            copy(kst.at[i], kret.at[i, y], kst_s.at[i], kret_r.at[i, y], partner).wait_recv()
         out = dk_out if i == 0 else dv_out
         for p in range(2):
-            for h in range(pair):
-                out[:, p * pair + h, :] = kret[i, p, :, h * width : (h + 1) * width]
+            out[:, p * lanes : (p + 1) * lanes] = kret[i, p]
     for p in range(2):
-        for h in range(pair):
-            dq_out[:, p * pair + h, :] = db[z, p, half_of(y), h * width : (h + 1) * width]
+        dq_out[:, p * lanes : (p + 1) * lanes] = db[z, p, half_of(y), :]
 
     def sent(c):
         c.wait_send()
@@ -853,16 +862,28 @@
         sent(swap(a))
     for own in (True, False):
         passes(sent, (Q, K, V, ST, G), own)
+    for a in (Q, ST, G):
+        @pl.when(z == high)
+        def _():
+            for half in range(2):
+                sent(relay(a, half))
     for level in range(nz):
         grad_each(level, sent)
     for i in range(2):
-        sent(return_copy(i))
+        @pl.when(z >= low)
+        def _():
+            sent(return_copy(i))
 
         @pl.when((z == low) | (z == high))
         def _():
             sent(part_copy(i))
 
         @pl.when(z == low)
+        def _():
+            for half in range(2):
+                sent(total_copy(i, half))
+
+        @pl.when(z < low)
         def _():
             sent(key_copy(i))
 
@@ -889,12 +910,12 @@
     block = (2 * rows, pair * width)
     half = (rows, pair * width)
     dma = pltpu.SemaphoreType.DMA
-    return pl.pallas_call(
+    dq, dk, dv, wg = pl.pallas_call(
         functools.partial(hub_kernel, nsp, ntp, heads, width),
         out_shape=(
-            jax.ShapeDtypeStruct(query_heads.shape, BF16),
-            jax.ShapeDtypeStruct(query_heads.shape, BF16),
-            jax.ShapeDtypeStruct(query_heads.shape, BF16),
+            jax.ShapeDtypeStruct(flat, BF16),
+            jax.ShapeDtypeStruct(flat, BF16),
+            jax.ShapeDtypeStruct(flat, BF16),
             jax.ShapeDtypeStruct((slab, heads * width), F32),
         ),
         in_specs=[pl.BlockSpec(memory_space=pltpu.SMEM)] + [vmem()] * 8,
@@ -916,8 +937,8 @@
             pltpu.VMEM((2,) + half, BF16),
             pltpu.VMEM((2, 2) + half, BF16),
             pltpu.VMEM((nsp, rows, slab), BF16),
-            dma((5,)), dma((2, 5, 2)), dma((4, nz, 2)), dma((nz, 2)), dma((nz, 3)), dma((nz, 2)),
-            dma((2,)), dma((2,)), dma, dma((2,)), dma((2,)), dma((2,)), dma((2,)),
+            dma((5,)), dma((5, 2)), dma((5, 2)), dma((4, nz, 2)), dma((nz, 2)), dma((nz, 3)), dma((nz, 2)),
+            dma((2,)), dma((2,)), dma, dma((2,)), dma((2,)), dma((2, 2)), dma((2,)), dma((2, 2)),
             dma((nsp,)), dma((nsp,)), dma((nsp, ntp)), dma((nsp, ntp)),
             dma,
         ],
@@ -932,8 +953,9 @@
         query_heads.reshape(flat),
         map_outputs,
         out_grad,
-        jnp.transpose(log_sums, (1, 0, 2)),
+        jnp.transpose(log_sums, (1, 2, 0)),
     )
+    return tuple(a.reshape(query_heads.shape) for a in (dq, dk, dv)) + (wg,)
 
 
 def solution(mesh):

time: 101 us -> 96.1 us (0.951)
  Pallas kernels: 88 us -> 85.3 us
  local copies, waits for them, and re-layouts: 11.6 us -> 9.78 us
    unnamed x8 -> x4, local copies, waits for them, and re-layouts: 9.7 us -> 2.66 us
    reshape x0 -> x3, local copies, waits for them, and re-layouts: none -> 5.24 us  [hub_body(): return tuple((a.reshape(query_heads.shape) for a in (dq, dk, dv))) + (wg,)]
    pallas_call x1, Pallas kernels: 88 us -> 85.3 us  [hub_body(): pl.pallas_call(functools.partial(hub_kernel, nsp, ntp, heads, width), out...]
where the time goes in v2:
time: 96.1 us; the launch traced here: 95.7 us
  Pallas kernels  85.3 us (89%)
  local copies, waits for them, and re-layouts  9.78 us (10%)
    pallas_call x1, Pallas kernels, hub_body(): pl.pallas_call(functools.partial(hub_kernel, nsp, ntp, heads, width), out...  85.3 us
    reshape x3, local copies, waits for them, and re-layouts, hub_body(): return tuple((a.reshape(query_heads.shape) for a in (dq, dk, dv))) + (wg,)  5.24 us
    unnamed x4, local copies, waits for them, and re-layouts  2.66 us

profile of v2, /device:TPU:0, one launch (start us, length us, event | category | flops | bytes accessed | tf_op | source)
XLA Modules:
  0.0 95.7 jit_solution(17990125100454426620)
XLA Ops:
  0.6 1.7 %copy.19 = bf16[32,8,4,128]{3,1,2,0:T(8,128)(2,1)} copy(bf16[32,8,4,128]{3,2,1,0:T(4,128)(2,1)} %bitcast.13) | data formatting | bytes 524288
  2.3 1.9 %copy_bitcast_fusion = (bf16[256,512]{1,0:T(8,128)(2,1)}, bf16[256,512]{1,0:T(8,128)(2,1)}) fusion(bf16[32,8,4,128]{3,2,1,0:T(4,128)(2,1)} %bitcast.14, bf16[32,8,4,128]{3,2,1,0:T(4,128)(2,1)} %bitcast.15), kind=kLoop, calls=%fused_computation | loop fusion | bytes 1048576 | tf_op jit(solution)/shard_map/reshape | solution.py:953
  4.2 85.3 %hub.1 = (bf16[256,512]{1,0:T(8,128)(2,1)}, bf16[256,512]{1,0:T(8,128)(2,1)}, bf16[256,512]{1,0:T(8,128)(2,1)}, f32[512,512]{1,0:T(8,128)}) custom-call(f32[4]{0:T(128)} %lam.1, f32[1,128]{1,0:T(1,128)} %bitcast.17, bf16[256,4096]{1,0:T(8,128)(2,1)} %lat.1, bf16[256,512]{1,0:T(8,128)(2,1)} %bitcast.12, bf16[256,512]{1,0:T(8,128)(2,1)} %get-tuple-element.13.own_v, ...), custom_call_target="tpu_custom_call" | custom-call | tf_op jit(solution)/shard_map/hub/pallas_call | solution.py:913
  89.5 0.0 copy-start
  89.5 1.8 %reshape.29 = bf16[256,4,128]{2,1,0:T(4,128)(2,1)} reshape(bf16[256,512]{1,0:T(8,128)(2,1)} %get-tuple-element.8) | data formatting | bytes 524288 | tf_op jit(solution)/shard_map/reshape | solution.py:958
  91.3 1.7 %reshape.30 = bf16[256,4,128]{2,1,0:T(4,128)(2,1)} reshape(bf16[256,512]{1,0:T(8,128)(2,1)} %get-tuple-element.9) | data formatting | bytes 524288 | tf_op jit(solution)/shard_map/reshape | solution.py:958
  93.0 1.7 %reshape.31 = bf16[256,4,128]{2,1,0:T(4,128)(2,1)} reshape(bf16[256,512]{1,0:T(8,128)(2,1)} %get-tuple-element.10) | data formatting | bytes 524288 | tf_op jit(solution)/shard_map/reshape | solution.py:958
  94.7 0.0 copy-done
  94.7 1.0 %copy.21 = f32[512,512]{1,0:T(8,128)} copy(f32[512,512]{1,0:T(8,128)S(1)} %copy-done) | data formatting | bytes 2097152
Async XLA Ops:
  89.5 5.3 %copy-start = (f32[512,512]{1,0:T(8,128)S(1)}, f32[512,512]{1,0:T(8,128)}, u32[]{:S(2)}) copy-start(f32[512,512]{1,0:T(8,128)} %get-tuple-element.21) | copy-start | bytes 3145732

commit v3 on v2

--- a/solution.py
+++ b/solution.py
@@ -469,11 +469,11 @@
         row_ref[h, 2:4] = jnp.transpose(terms)[0:2]
 
 
-def hub_kernel(nsp, ntp, heads, width, lam, gain, lat, own_k, own_v, own_q, mo, og, lse,
+def hub_kernel(nsp, ntp, heads, width, lam_far, gain_far, lat, own_k, own_v, own_q, mo_far, og_far, lse_far,
                dq_out, dk_out, dv_out, wg_out,
                own_g, row, blk, stb, dq_acc, dk_acc, dv_acc, db, out_b, in_b, in_a, kt, kin, kst, kret, latb,
                f_s, z_s, r_s, b_r, st_r, d_s, d_r, ob_s, ib_r, ia_r, kt_s, kin_r, tot_s, kst_s, kret_r,
-               la_s, la_r, lb_s, lb_r, own_sem):
+               la_s, la_r, lb_s, lb_r, own_sem, lam, gain, mo, og, lse, near):
     nz = nsp // 2
     low, high, top = nz // 2 - 1, nz // 2, nz - 1
     s = lax.axis_index("sp")
@@ -490,6 +490,13 @@
     partner = 2 * z + 1 - y
     Q, K, V, G, ST = range(5)
 
+    fetches = [
+        pltpu.make_async_copy(src, dst, near.at[i])
+        for i, (src, dst) in enumerate(((mo_far, mo), (og_far, og), (lse_far, lse), (gain_far, gain), (lam_far, lam)))
+    ]
+    for fetch in fetches:
+        fetch.start()
+
     barrier = pltpu.get_barrier_semaphore()
     for d in range(1, nsp):
         pl.semaphore_signal(barrier, inc=1, device_id={"sp": lax.rem(s + d, nsp)}, device_id_type=MESH)
@@ -569,18 +576,37 @@
         return pltpu.make_async_copy(
             lat.at[:, pl.ds(pl.multiple_of(s * slab, slab), slab)], latb.at[s], own_sem)
 
-    def share_copy(b, d):
-        mine = pl.ds(pl.multiple_of(t * part, part), part)
+    sides = ntp // 2
+    side, core = t // 2, lax.rem(t, 2)
+
+    def share_copy(b, k):
+        away = lax.rem(side + (k if k < sides else k - sides), sides)
+        quarter = t if k < sides else 2 * away + core
+        to = 2 * away + core if 0 < k < sides else 2 * side + 1 - core
+        at = pl.ds(pl.multiple_of(quarter * part, part), part)
         return pltpu.make_async_remote_copy(
-            src_ref=latb.at[b, mine, :], dst_ref=latb.at[b, mine, :],
-            send_sem=lb_s.at[b, d], recv_sem=lb_r.at[b, d],
-            device_id={"tp": lax.rem(t + d, ntp)}, device_id_type=MESH)
+            src_ref=latb.at[b, at, :], dst_ref=latb.at[b, at, :],
+            send_sem=lb_s.at[b, k], recv_sem=lb_r.at[b, quarter],
+            device_id={"tp": to}, device_id_type=MESH)
+
+    def share_arrive(b, quarter):
+        at = pl.ds(pl.multiple_of(quarter * part, part), part)
+        pltpu.make_async_remote_copy(
+            src_ref=latb.at[b, at, :], dst_ref=latb.at[b, at, :],
+            send_sem=lb_s.at[b, 0], recv_sem=lb_r.at[b, quarter],
+            device_id={"tp": 2 * side + 1 - core}, device_id_type=MESH).wait_recv()
 
     def group_of(src, dst, group):
         sz, dz = src // 2, dst // 2
-        first = (lax.rem(src, 2) == lax.rem(dst, 2)) & ((dz > sz) | ((dz < sz) & (sz < high)))
-        last = (sz >= high) & (dz < high)
-        return first if group == 0 else last if group == 2 else jnp.logical_not(first | last)
+        late = (sz >= high) & (dz < high)
+        upper = (sz >= high) & (dz >= high) & (dz < sz)
+        first = (lax.rem(src, 2) == lax.rem(dst, 2)) & ((dz > sz) | (sz < high))
+        if group == 3:
+            return late
+        if group == 2:
+            return upper
+        rest = jnp.logical_not(late | upper)
+        return rest & (first if group == 0 else jnp.logical_not(first))
 
     def lat_send(group):
         for d in range(1, nsp):
@@ -588,7 +614,7 @@
             def _():
                 lat_copy(d).start()
 
-    def lat_share(group):
+    def share_send(group):
         def step(d, carry):
             b = lax.rem(s + d, nsp)
 
@@ -596,10 +622,26 @@
             def _():
                 mine = pl.ds(pl.multiple_of(t * part, part), part)
                 copy(latb.at[b, mine, :], latb.at[b, mine, :], la_s.at[1], la_r.at[b], partner).wait_recv()
-                for e in range(1, ntp):
-                    share_copy(b, e).start()
+                for k in reversed(range(sides)):
+                    share_copy(b, k).start()
             return carry
         lax.fori_loop(1, nsp, step, 0)
+
+    def share_hand(group):
+        def hand(d, carry):
+            b = lax.rem(s + d, nsp)
+
+            @pl.when(group_of(b, s, group))
+            def _():
+                for k in range(sides + 1, 2 * sides):
+                    share_arrive(b, 2 * lax.rem(side + k - sides, sides) + core)
+                    share_copy(b, k).start()
+            return carry
+        lax.fori_loop(1, nsp, hand, 0)
+
+    def lat_share(group):
+        share_send(group)
+        share_hand(group)
 
     swap(Q).start()
     passes(start, (Q, K, V), True)
@@ -608,11 +650,14 @@
     lat_send(0)
     own_lat().start()
 
+    for fetch in fetches:
+        fetch.wait()
     row_norm_backward(heads, width, lam, gain, mo, og, lse, own_g, row)
 
     swap(G).start()
     swap(ST).start()
     passes(start, (ST, G), True)
+    lat_send(1)
 
     for a in (Q, K, V, G):
         blk[a, z, half_of(y), :] = owned[a][:, lane_of(y)]
@@ -675,16 +720,17 @@
         if lane == 0:
             to = partner
         elif lane == 1:
-            to = at_level(jnp.where(z == low, 0, jnp.where(z == high, top, low)))
+            down = high if level == 0 else 0
+            to = at_level(jnp.where(z == low, down, jnp.where(z == high, top, low)))
         else:
             to = at_level(high)
         return copy(db.at[level, y], db.at[level, y], d_s.at[level, lane], d_r.at[level, y], to)
 
     def grad_lanes(level):
-        chained = (z == high) | ((z == low) if level >= low else (z < low))
-        if level > low:
+        chained = (z <= high) if level == 0 else (z == high) | (z == low)
+        if level != low:
             return ((0, None), (1, chained))
-        return ((0, None), (1, chained), (2, z == level))
+        return ((0, None), (1, chained), (2, z == low))
 
     def grad_each(level, action):
         for lane, ok in reversed(grad_lanes(level)):
@@ -714,6 +760,20 @@
         return copy(kst.at[i], kret.at[i, y], kst_s.at[i], kret_r.at[i, y], partner)
 
     visit(z, z, 0, True)
+    relays((ST, G), 1 - y)
+
+    @pl.when(z >= high)
+    def _():
+        out_b[0] = dq_value(z).astype(BF16)
+
+    @pl.when(z == high)
+    def _():
+        part_copy(0).start()
+
+    @pl.when(z > high)
+    def _():
+        top_copy().start()
+        lat_send(2)
 
     @pl.when(z < low)
     def _():
@@ -723,20 +783,25 @@
             kt[i] = (dv_acc[0] if i else dk_acc[0] * score_scale).astype(BF16)
             key_copy(i).start()
 
-    @pl.when(z >= high)
-    def _():
-        out_b[0] = dq_value(z).astype(BF16)
-
-    @pl.when(z == high)
-    def _():
-        part_copy(0).start()
-
-    @pl.when(z > high)
-    def _():
-        top_copy().start()
-
-    lat_send(1)
-    lat_share(0)
+    def return_keys():
+        for i, acc, scale in ((0, dk_acc, score_scale), (1, dv_acc, 1.0)):
+            kst[i] = (acc[0, half_of(1 - y), :] * scale).astype(BF16)
+            return_copy(i).start()
+            kret[i, y] = (acc[0, half_of(y), :] * scale).astype(BF16)
+
+    def hand_on(level):
+        grad_arrive(level, y)
+        grad_each(level, start)
+
+    def total(level):
+        i = level - high
+        part_copy(i).wait_recv()
+        whole = dq_value(level) + in_b[i].astype(F32)
+        if level == top:
+            above = in_a[...].astype(F32)
+            whole = whole + jnp.where(z == high, above, jnp.zeros_like(above))
+        db[level, y] = whole.astype(BF16)
+        grad_each(level, start)
 
     @pl.when(z == low)
     def _():
@@ -762,24 +827,32 @@
             def _():
                 db[low, y] = dq_value(low).astype(BF16)
                 grad_each(low, start)
+                share_send(0)
 
             @pl.when((i > 0) & (kz == 1))
             def _():
                 out_b[qz - high] = dq_value(qz).astype(BF16)
                 part_copy(qz - high).start()
 
+            @pl.when((qz == high) & (kz == 1))
+            def _():
+                share_hand(0)
+
             @pl.when((qz == top) & (kz == 0))
             def _():
-                for j in range(2):
-                    key_copy(j).wait_recv()
-                    acc = dv_acc[1] if j else dk_acc[1] * score_scale
-                    kt[j] = (acc + kin[j].astype(F32)).astype(BF16)
-                    for half in range(2):
-                        total_copy(j, half).start()
+                hand_on(0)
             return carry
         lax.fori_loop(0, 5, step, 0)
-
-    relays((ST, G), 1 - y)
+        total(high)
+        total(top)
+        for j in range(2):
+            key_copy(j).wait_recv()
+            acc = dv_acc[1] if j else dk_acc[1] * score_scale
+            kt[j] = (acc + kin[j].astype(F32)).astype(BF16)
+            for half in range(2):
+                total_copy(j, half).start()
+        return_keys()
+        lat_share(1)
 
     @pl.when(z == high)
     def _():
@@ -787,53 +860,57 @@
         top_copy().wait_recv()
         out_b[1] = (dq_value(top) + in_a[...].astype(F32)).astype(BF16)
         part_copy(1).start()
-
-    lat_send(2)
-
-    @pl.when(z >= low)
-    def _():
-        for i, acc, scale in ((0, dk_acc, score_scale), (1, dv_acc, 1.0)):
-            kst[i] = (acc[0, half_of(1 - y), :] * scale).astype(BF16)
-            return_copy(i).start()
-            kret[i, y] = (acc[0, half_of(y), :] * scale).astype(BF16)
-
-    for level in (0, low):
-        @pl.when(z != level)
-        def _():
-            grad_arrive(level, y)
-            grad_each(level, start)
-
-    lat_share(1)
-
-    for level in (high, top):
-        i = level - high
-
-        @pl.when((z == low) | (z == high))
-        def _():
-            part_copy(i).wait_recv()
-            total = dq_value(level) + in_b[i].astype(F32)
-            if level == top:
-                above = in_a[...].astype(F32)
-                total = total + jnp.where(z == high, above, jnp.zeros_like(above))
-            db[level, y] = total.astype(BF16)
-
-        @pl.when((z != low) & (z != high))
-        def _():
-            grad_arrive(level, y)
-        grad_each(level, start)
-
-    lat_share(2)
-    own_lat().wait()
-
-    for level in range(nz):
+        return_keys()
+        lat_share(0)
+        hand_on(low)
+        lat_send(3)
+        hand_on(0)
+        total(high)
+        lat_share(1)
+        lat_share(2)
+        total(top)
+
+    @pl.when(z < low)
+    def _():
+        lat_share(0)
+        hand_on(low)
+        lat_share(1)
+
+    @pl.when(z > high)
+    def _():
+        return_keys()
+        lat_share(0)
+        hand_on(low)
+        lat_send(3)
+        hand_on(0)
+        lat_share(1)
+
+    def key_results():
+        for i in range(2):
+            copy(kst.at[i], kret.at[i, 1 - y], kst_s.at[i], kret_r.at[i, 1 - y], partner).wait_recv()
+
+            @pl.when(z < low)
+            def _():
+                copy(kst.at[i], kret.at[i, y], kst_s.at[i], kret_r.at[i, y], partner).wait_recv()
+            out = dv_out if i else dk_out
+            for p in range(2):
+                for h in range(pair):
+                    out[:, p * pair + h, :] = kret[i, p, :, h * width : (h + 1) * width]
+
+    def query_results():
+        for p in range(2):
+            for h in range(pair):
+                dq_out[:, p * pair + h, :] = db[z, p, half_of(y), h * width : (h + 1) * width]
+
+    def weights(level):
         grad_arrive(level, 1 - y)
         for half in range(2):
             b = 2 * level + half
 
             @pl.when(s != b)
             def _():
-                for e in range(1, ntp):
-                    share_copy(b, e).wait_recv()
+                for k in range(sides):
+                    share_arrive(b, 2 * lax.rem(side + k, sides) + 1 - core)
         feed = latb[2 * level : 2 * level + 2].reshape(span, slab)
         for p in range(2):
             at = slice(p * lanes, (p + 1) * lanes)
@@ -843,17 +920,34 @@
             else:
                 wg_out[:, at] += term
 
-    for i in range(2):
-        copy(kst.at[i], kret.at[i, 1 - y], kst_s.at[i], kret_r.at[i, 1 - y], partner).wait_recv()
-
-        @pl.when(z < low)
+    own_lat().wait()
+
+    @pl.when(z >= high)
+    def _():
+        key_results()
+
+    for level in range(high):
+        weights(level)
+
+        @pl.when((z < low) | (z > high))
         def _():
-            copy(kst.at[i], kret.at[i, y], kst_s.at[i], kret_r.at[i, y], partner).wait_recv()
-        out = dk_out if i == 0 else dv_out
-        for p in range(2):
-            out[:, p * lanes : (p + 1) * lanes] = kret[i, p]
-    for p in range(2):
-        dq_out[:, p * lanes : (p + 1) * lanes] = db[z, p, half_of(y), :]
+            hand_on(high + level)
+
+    @pl.when(z < high)
+    def _():
+        query_results()
+        lat_share(3)
+
+    for level in range(high, nz):
+        weights(level)
+
+    @pl.when(z < high)
+    def _():
+        key_results()
+
+    @pl.when(z >= high)
+    def _():
+        query_results()
 
     def sent(c):
         c.wait_send()
@@ -894,10 +988,20 @@
         sent(lat_copy(d))
 
     def drain(d, carry):
-        for e in range(1, ntp):
-            sent(share_copy(lax.rem(s + d, nsp), e))
+        for k in range(2 * sides):
+            if k != sides:
+                sent(share_copy(lax.rem(s + d, nsp), k))
         return carry
     lax.fori_loop(1, nsp, drain, 0)
+
+
+def finish_kernel(a, b, c, d, a_out, b_out, c_out, d_out):
+    for src, dst in ((a, a_out), (b, b_out), (c, c_out), (d, d_out)):
+        dst[...] = src[...]
+
+
+def far():
+    return pl.BlockSpec(memory_space=pltpu.HBM)
 
 
 def hub_body(nsp, ntp, latents, query_heads, key_heads, value_heads, map_outputs, log_sums, out_grad,
@@ -910,15 +1014,15 @@
     block = (2 * rows, pair * width)
     half = (rows, pair * width)
     dma = pltpu.SemaphoreType.DMA
-    dq, dk, dv, wg = pl.pallas_call(
+    results = pl.pallas_call(
         functools.partial(hub_kernel, nsp, ntp, heads, width),
         out_shape=(
-            jax.ShapeDtypeStruct(flat, BF16),
-            jax.ShapeDtypeStruct(flat, BF16),
-            jax.ShapeDtypeStruct(flat, BF16),
+            jax.ShapeDtypeStruct(query_heads.shape, BF16),
+            jax.ShapeDtypeStruct(query_heads.shape, BF16),
+            jax.ShapeDtypeStruct(query_heads.shape, BF16),
             jax.ShapeDtypeStruct((slab, heads * width), F32),
         ),
-        in_specs=[pl.BlockSpec(memory_space=pltpu.SMEM)] + [vmem()] * 8,
+        in_specs=[far()] * 3 + [vmem()] * 3 + [far()] * 3,
         out_specs=(vmem(),) * 4,
         scratch_shapes=[
             pltpu.VMEM(flat, BF16),
@@ -941,8 +1045,15 @@
             dma((2,)), dma((2,)), dma, dma((2,)), dma((2,)), dma((2, 2)), dma((2,)), dma((2, 2)),
             dma((nsp,)), dma((nsp,)), dma((nsp, ntp)), dma((nsp, ntp)),
             dma,
+            pltpu.SMEM(mix_lambda.shape, F32),
+            pltpu.VMEM((1, width), F32),
+            pltpu.VMEM(map_outputs.shape, BF16),
+            pltpu.VMEM(out_grad.shape, BF16),
+            pltpu.VMEM((heads, 2, rows), F32),
+            dma((5,)),
         ],
-        compiler_params=pltpu.CompilerParams(collective_id=0, has_side_effects=True),
+        compiler_params=pltpu.CompilerParams(
+            collective_id=0, has_side_effects=True, vmem_limit_bytes=54800000),
         name="hub",
     )(
         mix_lambda,
@@ -955,7 +1066,14 @@
         out_grad,
         jnp.transpose(log_sums, (1, 2, 0)),
     )
-    return tuple(a.reshape(query_heads.shape) for a in (dq, dk, dv)) + (wg,)
+    return pl.pallas_call(
+        finish_kernel,
+        out_shape=tuple(jax.ShapeDtypeStruct(a.shape, a.dtype) for a in results),
+        in_specs=[vmem()] * 4,
+        out_specs=(vmem(),) * 4,
+        compiler_params=pltpu.CompilerParams(vmem_limit_bytes=8 * 2**20),
+        name="finish",
+    )(*results)
 
 
 def solution(mesh):

time: 96.1 us -> 83.2 us (0.87)
  Pallas kernels: 85.3 us -> 77 us
  local copies, waits for them, and re-layouts: 9.78 us -> 5.3 us
    pallas_call x1, Pallas kernels: 85.3 us -> 75.6 us  [hub_body(): pl.pallas_call(functools.partial(hub_kernel, nsp, ntp, heads, width), out...]
    reshape x3 -> x0, local copies, waits for them, and re-layouts: 5.24 us -> none  [hub_body(): return tuple((a.reshape(query_heads.shape) for a in (dq, dk, dv))) + (wg,)]
    unnamed x4 -> x9, local copies, waits for them, and re-layouts: 2.66 us -> 4.21 us
    pallas_call x0 -> x1, Pallas kernels: none -> 1.35 us  [hub_body(): pl.pallas_call(finish_kernel, out_shape=tuple((jax.ShapeDtypeStruct(a.sha...]
where the time goes in v3:
time: 83.2 us; the launch traced here: 82.9 us
  Pallas kernels  77 us (93%)
  local copies, waits for them, and re-layouts  5.3 us (6%)
    pallas_call x1, Pallas kernels, hub_body(): pl.pallas_call(functools.partial(hub_kernel, nsp, ntp, heads, width), out...  75.6 us
    unnamed x9, local copies, waits for them, and re-layouts  4.21 us

profile of v3, /device:TPU:0, one launch (start us, length us, event | category | flops | bytes accessed | tf_op | source)
XLA Modules:
  0.0 82.9 jit_solution(16358917529710969822)
XLA Ops:
  0.6 1.0 %copy.19 = bf16[32,8,4,128]{3,1,2,0:T(8,128)(2,1)S(1)} copy(bf16[32,8,4,128]{3,2,1,0:T(4,128)(2,1)} %bitcast.15) | data formatting | bytes 524288
  1.6 1.1 %copy_bitcast_fusion = (bf16[256,512]{1,0:T(8,128)(2,1)S(1)}, bf16[256,512]{1,0:T(8,128)(2,1)S(1)}) fusion(bf16[32,8,4,128]{3,2,1,0:T(4,128)(2,1)} %bitcast.16, bf16[32,8,4,128]{3,2,1,0:T(4,128)(2,1)} %bitcast.17), kind=kLoop, calls=%fused_computation | loop fusion | bytes 1048576 | tf_op jit(solution)/shard_map/reshape | solution.py:1064
  2.7 0.0 copy-start.1
  2.7 0.7 copy-done.1
  3.4 0.0 copy-start.2
  3.4 0.7 copy-done.2
  4.1 0.0 copy-start.3
  4.1 0.7 copy-done.3
  4.7 75.6 %hub.1 = (bf16[256,4,128]{2,1,0:T(4,128)(2,1)S(1)}, bf16[256,4,128]{2,1,0:T(4,128)(2,1)S(1)}, bf16[256,4,128]{2,1,0:T(4,128)(2,1)S(1)}, f32[512,512]{1,0:T(8,128)}) custom-call(f32[4]{0:T(128)S(1)} %copy-done.2, f32[1,128]{1,0:T(1,128)S(1)} %bitcast.14, bf16[256,4096]{1,0:T(8,128)(2,1)} %lat.1, bf16[256,512]{1,0:T(8,128)(2,1)S(1)} %bitcast.12, ...), custom_call_target="tpu_custom_call" | custom-call | tf_op jit(solution)/shard_map/hub/pallas_call | solution.py:1017
  80.4 0.0 copy-start
  80.4 1.2 %copy-done = f32[512,512]{1,0:T(8,128)S(1)} copy-done((f32[512,512]{1,0:T(8,128)S(1)}, f32[512,512]{1,0:T(8,128)}, u32[]{:S(2)}) %copy-start) | copy-done | bytes 1048600
  81.6 1.3 %finish.1 = (bf16[256,4,128]{2,1,0:T(4,128)(2,1)}, bf16[256,4,128]{2,1,0:T(4,128)(2,1)}, bf16[256,4,128]{2,1,0:T(4,128)(2,1)}, f32[512,512]{1,0:T(8,128)}) custom-call(bf16[256,4,128]{2,1,0:T(4,128)(2,1)S(1)} %get-tuple-element.8.a, bf16[256,4,128]{2,1,0:T(4,128)(2,1)S(1)} %get-tuple-element.9.b, bf16[256,4,128]{2,1,0:T(4,128)(2,1)S(1)} %get-tuple-element.10.c, ...), custom_call_target="tpu_custom_call" | custom-call | tf_op jit(solution)/shard_map/finish/pallas_call | solution.py:1069
Async XLA Ops:
  2.7 0.7 copy-start.1
  3.4 0.7 copy-start.2
  4.1 0.7 copy-start.3
  80.4 1.2 %copy-start = (f32[512,512]{1,0:T(8,128)S(1)}, f32[512,512]{1,0:T(8,128)}, u32[]{:S(2)}) copy-start(f32[512,512]{1,0:T(8,128)} %get-tuple-element.11.d) | copy-start | bytes 3145732

commit v4 on v3

--- a/solution.py
+++ b/solution.py
@@ -446,34 +446,34 @@
     return dq, dk, dv, wg
 
 
-def row_norm_backward(heads, width, lam_ref, gain_ref, mo_ref, og_ref, lse_ref, grad_ref, row_ref):
+def row_norm_backward(heads, width, small, maps, grad_ref, row_ref):
+    count = maps.shape[0]
     for h in range(heads):
-        first = mo_ref[:, 0, h, :].astype(F32)
-        second = mo_ref[:, 1, h, :].astype(F32)
-        lam = lam_ref[h]
+        first = maps[:, 0, h, :].astype(F32)
+        second = maps[:, 1, h, :].astype(F32)
+        lam = small[heads, 1:2, h : h + 1]
         combined = first - lam * second
         inverse = lax.rsqrt(jnp.mean(combined * combined, axis=-1, keepdims=True) + EPSILON)
-        weighted = gain_ref[...] * og_ref[:, h, :].astype(F32)
+        weighted = small[heads, 0:1, :width] * maps[:, 2, h, :].astype(F32)
         grad = (
             inverse * weighted
             - inverse**3 * combined * jnp.mean(combined * weighted, axis=-1, keepdims=True)
         ).astype(BF16)
         grad_ref[:, h * width : (h + 1) * width] = grad
         wide = grad.astype(F32)
-        log_lam = jnp.log(jnp.full((1, 1), lam, F32)) * LOG2E
-        row_ref[h, 0:1] = lse_ref[h, 0:1] * LOG2E
-        row_ref[h, 1:2] = lse_ref[h, 1:2] * LOG2E - log_lam
+        row_ref[h, 0:1] = small[h, 0:1, :count] * LOG2E
+        row_ref[h, 1:2] = small[h, 1:2, :count] * LOG2E - jnp.log(lam) * LOG2E
         lane = lax.broadcasted_iota(jnp.int32, wide.shape, 1)
         terms = jnp.where(lane == 0, jnp.sum(wide * first, axis=-1, keepdims=True),
                           jnp.sum(wide * second, axis=-1, keepdims=True))
         row_ref[h, 2:4] = jnp.transpose(terms)[0:2]
 
 
-def hub_kernel(nsp, ntp, heads, width, lam_far, gain_far, lat, own_k, own_v, own_q, mo_far, og_far, lse_far,
+def hub_kernel(nsp, ntp, heads, width, small, lat, own_k, own_v, own_q, maps,
                dq_out, dk_out, dv_out, wg_out,
                own_g, row, blk, stb, dq_acc, dk_acc, dv_acc, db, out_b, in_b, in_a, kt, kin, kst, kret, latb,
                f_s, z_s, r_s, b_r, st_r, d_s, d_r, ob_s, ib_r, ia_r, kt_s, kin_r, tot_s, kst_s, kret_r,
-               la_s, la_r, lb_s, lb_r, own_sem, lam, gain, mo, og, lse, near):
+               la_s, la_r, lb_s, lb_r, own_sem):
     nz = nsp // 2
     low, high, top = nz // 2 - 1, nz // 2, nz - 1
     s = lax.axis_index("sp")
@@ -490,13 +490,6 @@
     partner = 2 * z + 1 - y
     Q, K, V, G, ST = range(5)
 
-    fetches = [
-        pltpu.make_async_copy(src, dst, near.at[i])
-        for i, (src, dst) in enumerate(((mo_far, mo), (og_far, og), (lse_far, lse), (gain_far, gain), (lam_far, lam)))
-    ]
-    for fetch in fetches:
-        fetch.start()
-
     barrier = pltpu.get_barrier_semaphore()
     for d in range(1, nsp):
         pl.semaphore_signal(barrier, inc=1, device_id={"sp": lax.rem(s + d, nsp)}, device_id_type=MESH)
@@ -601,8 +594,8 @@
         late = (sz >= high) & (dz < high)
         upper = (sz >= high) & (dz >= high) & (dz < sz)
         first = (lax.rem(src, 2) == lax.rem(dst, 2)) & ((dz > sz) | (sz < high))
-        if group == 3:
-            return late
+        if group >= 3:
+            return late & ((dz < low) if group == 3 else (dz >= low))
         if group == 2:
             return upper
         rest = jnp.logical_not(late | upper)
@@ -647,17 +640,16 @@
     passes(start, (Q, K, V), True)
     swap(K).start()
     swap(V).start()
-    lat_send(0)
+    @pl.when(z >= low)
+    def _():
+        lat_send(0)
     own_lat().start()
 
-    for fetch in fetches:
-        fetch.wait()
-    row_norm_backward(heads, width, lam, gain, mo, og, lse, own_g, row)
+    row_norm_backward(heads, width, small, maps, own_g, row)
 
     swap(G).start()
     swap(ST).start()
     passes(start, (ST, G), True)
-    lat_send(1)
 
     for a in (Q, K, V, G):
         blk[a, z, half_of(y), :] = owned[a][:, lane_of(y)]
@@ -671,9 +663,15 @@
         passes(start, (a,), False)
         if a == Q:
             relays((Q,), y)
-        if a == G:
+        if a == K:
+            relays((ST, G), y)
+        if a == V:
             relays((Q,), 1 - y)
-            relays((ST, G), y)
+
+            @pl.when(z < low)
+            def _():
+                lat_send(0)
+
 
     lane_id = lax.broadcasted_iota(jnp.int32, (1, width), 1)
     first_map = jnp.where(lane_id < width // 2, 1.0, 0.0).astype(BF16)
@@ -713,10 +711,11 @@
             return carry
         lax.fori_loop(0, pair, one, 0)
 
-    def dq_value(level):
-        return jnp.concatenate([jnp.transpose(dq_acc[level, h]) for h in range(pair)], axis=1) * score_scale
-
-    def grad_copy(level, lane):
+    def dq_value(level, c):
+        at = pl.ds(c * rows, rows)
+        return jnp.concatenate([jnp.transpose(dq_acc[level, h, :, at]) for h in range(pair)], axis=1) * score_scale
+
+    def grad_copy(level, lane, c):
         if lane == 0:
             to = partner
         elif lane == 1:
@@ -724,7 +723,8 @@
             to = at_level(jnp.where(z == low, down, jnp.where(z == high, top, low)))
         else:
             to = at_level(high)
-        return copy(db.at[level, y], db.at[level, y], d_s.at[level, lane], d_r.at[level, y], to)
+        piece = db.at[level, y, half_of(c), :]
+        return copy(piece, piece, d_s.at[level, lane, c], d_r.at[level, y, c], to)
 
     def grad_lanes(level):
         chained = (z <= high) if level == 0 else (z == high) | (z == low)
@@ -732,23 +732,31 @@
             return ((0, None), (1, chained))
         return ((0, None), (1, chained), (2, z == low))
 
-    def grad_each(level, action):
-        for lane, ok in reversed(grad_lanes(level)):
-            if ok is None:
-                action(grad_copy(level, lane))
-            else:
-                @pl.when(ok)
-                def _():
-                    action(grad_copy(level, lane))
-
-    def grad_arrive(level, p):
-        copy(db.at[level, p], db.at[level, p], d_s.at[level, 0], d_r.at[level, p], partner).wait_recv()
-
-    def part_copy(i):
-        return copy(out_b.at[i], in_b.at[i], ob_s.at[i], ib_r.at[i], at_level(jnp.where(z == low, high, low)))
-
-    def top_copy():
-        return copy(out_b.at[0], in_a, ob_s.at[0], ia_r, at_level(high))
+    def grad_each(level, action, chunks=(0, 1), only=(0, 1, 2)):
+        for c in chunks:
+            for lane, ok in reversed(grad_lanes(level)):
+                if lane not in only:
+                    continue
+                if ok is None:
+                    action(grad_copy(level, lane, c))
+                else:
+                    @pl.when(ok)
+                    def _():
+                        action(grad_copy(level, lane, c))
+
+    def grad_arrive(level, p, c):
+        piece = db.at[level, p, half_of(c), :]
+        copy(piece, piece, d_s.at[level, 0, c], d_r.at[level, p, c], partner).wait_recv()
+
+    def part_copy(i, c):
+        return copy(out_b.at[i, half_of(c), :], in_b.at[i, half_of(c), :], ob_s.at[i, c], ib_r.at[i, c],
+                    at_level(jnp.where(z == low, high, low)))
+
+    def top_copy(c):
+        return copy(out_b.at[0, half_of(c), :], in_a.at[half_of(c), :], ob_s.at[0, c], ia_r.at[c], at_level(high))
+
+    def rows_of(c):
+        return slice(c * rows, (c + 1) * rows)
 
     def key_copy(i):
         return copy(kt.at[i], kin.at[i], kt_s.at[i], kin_r.at[i], at_level(low))
@@ -759,29 +767,40 @@
     def return_copy(i):
         return copy(kst.at[i], kret.at[i, y], kst_s.at[i], kret_r.at[i, y], partner)
 
+    @pl.when(z >= low)
+    def _():
+        lat_send(1)
+
     visit(z, z, 0, True)
     relays((ST, G), 1 - y)
 
     @pl.when(z >= high)
     def _():
-        out_b[0] = dq_value(z).astype(BF16)
+        for c in range(2):
+            out_b[0, rows_of(c)] = dq_value(z, c).astype(BF16)
 
     @pl.when(z == high)
     def _():
-        part_copy(0).start()
+        lat_send(3)
+        for c in range(2):
+            part_copy(0, c).start()
 
     @pl.when(z > high)
     def _():
-        top_copy().start()
+        for c in range(2):
+            top_copy(c).start()
+        lat_send(3)
         lat_send(2)
 
     @pl.when(z < low)
     def _():
-        db[0, y] = dq_value(0).astype(BF16)
+        for c in range(2):
+            db[0, y, rows_of(c)] = dq_value(0, c).astype(BF16)
         grad_each(0, start)
         for i in range(2):
             kt[i] = (dv_acc[0] if i else dk_acc[0] * score_scale).astype(BF16)
             key_copy(i).start()
+        lat_send(1)
 
     def return_keys():
         for i, acc, scale in ((0, dk_acc, score_scale), (1, dv_acc, 1.0)):
@@ -790,103 +809,23 @@
             kret[i, y] = (acc[0, half_of(y), :] * scale).astype(BF16)
 
     def hand_on(level):
-        grad_arrive(level, y)
-        grad_each(level, start)
+        for c in range(2):
+            grad_arrive(level, y, c)
+            grad_each(level, start, (c,))
 
     def total(level):
         i = level - high
-        part_copy(i).wait_recv()
-        whole = dq_value(level) + in_b[i].astype(F32)
-        if level == top:
-            above = in_a[...].astype(F32)
-            whole = whole + jnp.where(z == high, above, jnp.zeros_like(above))
-        db[level, y] = whole.astype(BF16)
-        grad_each(level, start)
-
-    @pl.when(z == low)
-    def _():
-        def step(i, carry):
-            qz = jnp.where(i == 0, low, high + (i - 1) // 2)
-            kz = jnp.where(i == 0, 0, lax.rem(i - 1, 2))
-
-            @pl.when(i == 0)
-            def _():
-                for half in range(2):
-                    arrive(K, 0, half)
-                    arrive(V, 0, half)
-
-            @pl.when((i > 0) & (kz == 0))
-            def _():
-                for a in (Q, ST, G):
-                    for half in range(2):
-                        arrive(a, qz, half)
-
-            visit(qz, kz, 1 - kz, False)
-
-            @pl.when(i == 0)
-            def _():
-                db[low, y] = dq_value(low).astype(BF16)
-                grad_each(low, start)
-                share_send(0)
-
-            @pl.when((i > 0) & (kz == 1))
-            def _():
-                out_b[qz - high] = dq_value(qz).astype(BF16)
-                part_copy(qz - high).start()
-
-            @pl.when((qz == high) & (kz == 1))
-            def _():
-                share_hand(0)
-
-            @pl.when((qz == top) & (kz == 0))
-            def _():
-                hand_on(0)
-            return carry
-        lax.fori_loop(0, 5, step, 0)
-        total(high)
-        total(top)
-        for j in range(2):
-            key_copy(j).wait_recv()
-            acc = dv_acc[1] if j else dk_acc[1] * score_scale
-            kt[j] = (acc + kin[j].astype(F32)).astype(BF16)
-            for half in range(2):
-                total_copy(j, half).start()
-        return_keys()
-        lat_share(1)
-
-    @pl.when(z == high)
-    def _():
-        visit(top, high, 0, False)
-        top_copy().wait_recv()
-        out_b[1] = (dq_value(top) + in_a[...].astype(F32)).astype(BF16)
-        part_copy(1).start()
-        return_keys()
-        lat_share(0)
-        hand_on(low)
-        lat_send(3)
-        hand_on(0)
-        total(high)
-        lat_share(1)
-        lat_share(2)
-        total(top)
-
-    @pl.when(z < low)
-    def _():
-        lat_share(0)
-        hand_on(low)
-        lat_share(1)
-
-    @pl.when(z > high)
-    def _():
-        return_keys()
-        lat_share(0)
-        hand_on(low)
-        lat_send(3)
-        hand_on(0)
-        lat_share(1)
-
-    def key_results():
-        for i in range(2):
+        for c in range(2):
+            part_copy(i, c).wait_recv()
+            whole = dq_value(level, c) + in_b[i, rows_of(c)].astype(F32)
+            if level == top:
+                above = in_a[rows_of(c)].astype(F32)
+                whole = whole + jnp.where(z == high, above, jnp.zeros_like(above))
+            db[level, y, rows_of(c)] = whole.astype(BF16)
+            grad_each(level, start, (c,))
+
+    def key_results(which=(0, 1)):
+        for i in which:
             copy(kst.at[i], kret.at[i, 1 - y], kst_s.at[i], kret_r.at[i, 1 - y], partner).wait_recv()
 
             @pl.when(z < low)
@@ -903,7 +842,8 @@
                 dq_out[:, p * pair + h, :] = db[z, p, half_of(y), h * width : (h + 1) * width]
 
     def weights(level):
-        grad_arrive(level, 1 - y)
+        for c in range(2):
+            grad_arrive(level, 1 - y, c)
         for half in range(2):
             b = 2 * level + half
 
@@ -920,37 +860,147 @@
             else:
                 wg_out[:, at] += term
 
+    @pl.when(z == low)
+    def _():
+        def step(i, carry):
+            qz = jnp.where(i == 0, low, high + (i - 1) // 2)
+            kz = jnp.where(i == 0, 0, lax.rem(i - 1, 2))
+
+            @pl.when(i == 0)
+            def _():
+                for half in range(2):
+                    arrive(K, 0, half)
+                    arrive(V, 0, half)
+
+            @pl.when((i > 0) & (kz == 0))
+            def _():
+                for a in (Q, ST, G):
+                    for half in range(2):
+                        arrive(a, qz, half)
+
+            visit(qz, kz, 1 - kz, False)
+
+            @pl.when(i == 0)
+            def _():
+                for c in range(2):
+                    db[low, y, rows_of(c)] = dq_value(low, c).astype(BF16)
+                grad_each(low, start)
+                share_send(0)
+
+            @pl.when((i > 0) & (kz == 1))
+            def _():
+                for c in range(2):
+                    out_b[qz - high, rows_of(c)] = dq_value(qz, c).astype(BF16)
+                    part_copy(qz - high, c).start()
+
+            @pl.when((qz == high) & (kz == 1))
+            def _():
+                share_hand(0)
+
+            @pl.when((qz == top) & (kz == 0))
+            def _():
+                for c in range(2):
+                    grad_arrive(0, y, c)
+                grad_each(0, start, only=(0,))
+            return carry
+        lax.fori_loop(0, 5, step, 0)
+        grad_each(0, start, only=(1,))
+        return_keys()
+
+        def key_total(j):
+            key_copy(j).wait_recv()
+            acc = dv_acc[1] if j else dk_acc[1] * score_scale
+            kt[j] = (acc + kin[j].astype(F32)).astype(BF16)
+            for half in range(2):
+                total_copy(j, half).start()
+
+        key_total(0)
+        total(high)
+        total(top)
+        key_total(1)
+        lat_share(1)
+
+    @pl.when(z == high)
+    def _():
+        visit(top, high, 0, False)
+        for c in range(2):
+            top_copy(c).wait_recv()
+            out_b[1, rows_of(c)] = (dq_value(top, c) + in_a[rows_of(c)].astype(F32)).astype(BF16)
+            part_copy(1, c).start()
+        return_keys()
+        share_send(0)
+        hand_on(low)
+        share_hand(0)
+        total(high)
+        lat_send(4)
+        share_send(2)
+        key_results()
+        share_hand(2)
+        total(top)
+        hand_on(0)
+        share_send(1)
+        share_hand(1)
+
+    @pl.when(z < low)
+    def _():
+        share_send(0)
+        hand_on(low)
+        share_hand(0)
+        share_send(1)
+        share_hand(1)
+        share_send(3)
+        share_hand(3)
+
+    @pl.when(z > high)
+    def _():
+        return_keys()
+        share_send(0)
+        hand_on(low)
+        share_hand(0)
+        key_results()
+        lat_send(4)
+        hand_on(high)
+        hand_on(top)
+        hand_on(0)
+        share_send(1)
+        share_hand(1)
+
     own_lat().wait()
-
-    @pl.when(z >= high)
-    def _():
-        key_results()
-
     for level in range(high):
         weights(level)
 
-        @pl.when((z < low) | (z > high))
+        @pl.when(z < low)
         def _():
             hand_on(high + level)
 
     @pl.when(z < high)
     def _():
         query_results()
-        lat_share(3)
+        share_send(4)
+
+        @pl.when(z == low)
+        def _():
+            key_results()
+
+        @pl.when(z < low)
+        def _():
+            key_results((0,))
+        share_hand(4)
 
     for level in range(high, nz):
         weights(level)
 
-    @pl.when(z < high)
-    def _():
-        key_results()
-
-    @pl.when(z >= high)
-    def _():
-        query_results()
+        @pl.when(z == level)
+        def _():
+            query_results()
+
+    @pl.when(z < low)
+    def _():
+        key_results((1,))
 
     def sent(c):
         c.wait_send()
+
 
     for a in range(5):
         sent(swap(a))
@@ -970,7 +1020,8 @@
 
         @pl.when((z == low) | (z == high))
         def _():
-            sent(part_copy(i))
+            for c in range(2):
+                sent(part_copy(i, c))
 
         @pl.when(z == low)
         def _():
@@ -983,7 +1034,8 @@
 
     @pl.when(z > high)
     def _():
-        sent(top_copy())
+        for c in range(2):
+            sent(top_copy(c))
     for d in range(1, nsp):
         sent(lat_copy(d))
 
@@ -995,9 +1047,15 @@
     lax.fori_loop(1, nsp, drain, 0)
 
 
-def finish_kernel(a, b, c, d, a_out, b_out, c_out, d_out):
-    for src, dst in ((a, a_out), (b, b_out), (c, c_out), (d, d_out)):
-        dst[...] = src[...]
+def finish_kernel(a, b, c, d, a_out, b_out, c_out, d_out, sems):
+    stores = [
+        pltpu.make_async_copy(src, dst, sems.at[i])
+        for i, (src, dst) in enumerate(((a, a_out), (b, b_out), (c, c_out), (d, d_out)))
+    ]
+    for store in stores:
+        store.start()
+    for store in stores:
+        store.wait()
 
 
 def far():
@@ -1014,6 +1072,14 @@
     block = (2 * rows, pair * width)
     half = (rows, pair * width)
     dma = pltpu.SemaphoreType.DMA
+    room = max(rows, width, heads)
+
+    sums = jnp.transpose(log_sums, (1, 2, 0))
+    small = (
+        jnp.pad(sums, ((0, 1), (0, 0), (0, room - rows)))
+        + jnp.pad(norm_gain[None, None, :], ((heads, 0), (0, 1), (0, room - width)))
+        + jnp.pad(mix_lambda[None, None, :], ((heads, 0), (1, 0), (0, room - heads)))
+    )
     results = pl.pallas_call(
         functools.partial(hub_kernel, nsp, ntp, heads, width),
         out_shape=(
@@ -1022,7 +1088,7 @@
             jax.ShapeDtypeStruct(query_heads.shape, BF16),
             jax.ShapeDtypeStruct((slab, heads * width), F32),
         ),
-        in_specs=[far()] * 3 + [vmem()] * 3 + [far()] * 3,
+        in_specs=[vmem(), far()] + [vmem()] * 4,
         out_specs=(vmem(),) * 4,
         scratch_shapes=[
             pltpu.VMEM(flat, BF16),
@@ -1041,37 +1107,29 @@
             pltpu.VMEM((2,) + half, BF16),
             pltpu.VMEM((2, 2) + half, BF16),
             pltpu.VMEM((nsp, rows, slab), BF16),
-            dma((5,)), dma((5, 2)), dma((5, 2)), dma((4, nz, 2)), dma((nz, 2)), dma((nz, 3)), dma((nz, 2)),
-            dma((2,)), dma((2,)), dma, dma((2,)), dma((2,)), dma((2, 2)), dma((2,)), dma((2, 2)),
+            dma((5,)), dma((5, 2)), dma((5, 2)), dma((4, nz, 2)), dma((nz, 2)), dma((nz, 3, 2)), dma((nz, 2, 2)),
+            dma((2, 2)), dma((2, 2)), dma((2,)), dma((2,)), dma((2,)), dma((2, 2)), dma((2,)), dma((2, 2)),
             dma((nsp,)), dma((nsp,)), dma((nsp, ntp)), dma((nsp, ntp)),
             dma,
-            pltpu.SMEM(mix_lambda.shape, F32),
-            pltpu.VMEM((1, width), F32),
-            pltpu.VMEM(map_outputs.shape, BF16),
-            pltpu.VMEM(out_grad.shape, BF16),
-            pltpu.VMEM((heads, 2, rows), F32),
-            dma((5,)),
         ],
         compiler_params=pltpu.CompilerParams(
-            collective_id=0, has_side_effects=True, vmem_limit_bytes=54800000),
+            collective_id=0, has_side_effects=True, vmem_limit_bytes=52500000),
         name="hub",
     )(
-        mix_lambda,
-        norm_gain[None, :],
+        small,
         latents,
         key_heads.reshape(flat),
         value_heads.reshape(flat),
         query_heads.reshape(flat),
-        map_outputs,
-        out_grad,
-        jnp.transpose(log_sums, (1, 2, 0)),
+        jnp.concatenate([map_outputs, out_grad[:, None]], axis=1),
     )
     return pl.pallas_call(
         finish_kernel,
         out_shape=tuple(jax.ShapeDtypeStruct(a.shape, a.dtype) for a in results),
         in_specs=[vmem()] * 4,
-        out_specs=(vmem(),) * 4,
-        compiler_params=pltpu.CompilerParams(vmem_limit_bytes=8 * 2**20),
+        out_specs=(far(),) * 4,
+        scratch_shapes=[pltpu.SemaphoreType.DMA((4,))],
+        compiler_params=pltpu.CompilerParams(vmem_limit_bytes=52500000),
         name="finish",
     )(*results)
 

time: 83.2 us -> 75.8 us (0.911); the launches traced: 82.9 us -> 74.3 us
  Pallas kernels: 77 us -> 69 us
  local copies, waits for them, and re-layouts: 5.3 us -> 2.08 us
  other arithmetic: 0 us -> 2.41 us
    pallas_call x1, Pallas kernels: 75.6 us -> 67.7 us  [hub_body(): pl.pallas_call(functools.partial(hub_kernel, nsp, ntp, heads, width), out...]
    unnamed x9 -> x1, local copies, waits for them, and re-layouts: 4.21 us -> 0.99 us
    concatenate x0 -> x1, other arithmetic: none -> 1.67 us  [hub_body(): jnp.concatenate([map_outputs, out_grad[:, None]], axis=1)]
where the time goes in v4:
time: 75.8 us; the launch traced here: 74.3 us
  Pallas kernels  69 us (91%)
  other arithmetic  2.41 us (3%)
  local copies, waits for them, and re-layouts  2.08 us (3%)
  between operations  0.83 us (1%)
    pallas_call x1, Pallas kernels, hub_body(): pl.pallas_call(functools.partial(hub_kernel, nsp, ntp, heads, width), out...  67.7 us
    concatenate x1, other arithmetic, hub_body(): jnp.concatenate([map_outputs, out_grad[:, None]], axis=1)  1.67 us

profile of v4, /device:TPU:0, one launch (start us, length us, event | category | flops | bytes accessed | tf_op | source)
XLA Modules:
  0.0 74.3 jit_solution(13564481317468103108)
XLA Ops:
  0.6 0.7 pad_add_fusion.small
  1.4 1.0 %copy.19 = bf16[32,8,4,128]{3,1,2,0:T(8,128)(2,1)S(1)} copy(bf16[32,8,4,128]{3,2,1,0:T(4,128)(2,1)} %bitcast.15) | data formatting | bytes 524288
  2.4 1.1 %copy_bitcast_fusion = (bf16[256,512]{1,0:T(8,128)(2,1)S(1)}, bf16[256,512]{1,0:T(8,128)(2,1)S(1)}) fusion(bf16[32,8,4,128]{3,2,1,0:T(4,128)(2,1)} %bitcast.16, bf16[32,8,4,128]{3,2,1,0:T(4,128)(2,1)} %bitcast.17), kind=kLoop, calls=%fused_computation.1 | loop fusion | bytes 1048576 | tf_op jit(solution)/shard_map/reshape | solution.py:1123
  3.5 1.7 %pad_maximum_fusion.maps = bf16[256,3,4,128]{3,2,1,0:T(4,128)(2,1)S(1)} fusion(bf16[256,1,4,128]{3,2,1,0:T(4,128)(2,1)} %bitcast.18, bf16[256,2,4,128]{3,2,1,0:T(4,128)(2,1)} %param.13), kind=kLoop, calls=%fused_computation | loop fusion | flops 393216 | bytes 1572864 | tf_op jit(solution)/shard_map/concatenate | solution.py:1124
  5.1 67.7 %hub.1 = (bf16[256,4,128]{2,1,0:T(4,128)(2,1)S(1)}, bf16[256,4,128]{2,1,0:T(4,128)(2,1)S(1)}, bf16[256,4,128]{2,1,0:T(4,128)(2,1)S(1)}, f32[512,512]{1,0:T(8,128)S(1)}) custom-call(f32[5,2,256]{2,1,0:T(2,128)S(1)} %pad_add_fusion.small, bf16[256,4096]{1,0:T(8,128)(2,1)} %lat.1, bf16[256,512]{1,0:T(8,128)(2,1)S(1)} %bitcast.14, ...), custom_call_target="tpu_custom_call" | custom-call | tf_op jit(solution)/shard_map/hub/pallas_call | solution.py:1083
  72.9 1.3 %finish.1 = (bf16[256,4,128]{2,1,0:T(4,128)(2,1)}, bf16[256,4,128]{2,1,0:T(4,128)(2,1)}, bf16[256,4,128]{2,1,0:T(4,128)(2,1)}, f32[512,512]{1,0:T(8,128)}) custom-call(bf16[256,4,128]{2,1,0:T(4,128)(2,1)S(1)} %get-tuple-element.8.a, bf16[256,4,128]{2,1,0:T(4,128)(2,1)S(1)} %get-tuple-element.9.b, bf16[256,4,128]{2,1,0:T(4,128)(2,1)S(1)} %get-tuple-element.10.c, ...), custom_call_target="tpu_custom_call" | custom-call | tf_op jit(solution)/shard_map/finish/pallas_call | solution.py:1126

commit v5 on v4

--- a/solution.py
+++ b/solution.py
@@ -594,12 +594,14 @@
         late = (sz >= high) & (dz < high)
         upper = (sz >= high) & (dz >= high) & (dz < sz)
         first = (lax.rem(src, 2) == lax.rem(dst, 2)) & ((dz > sz) | (sz < high))
-        if group >= 3:
+        if group in (3, 4):
             return late & ((dz < low) if group == 3 else (dz >= low))
         if group == 2:
             return upper
         rest = jnp.logical_not(late | upper)
-        return rest & (first if group == 0 else jnp.logical_not(first))
+        if group == 0:
+            return rest & first
+        return rest & jnp.logical_not(first) & ((sz >= low) if group == 1 else (sz < low))
 
     def lat_send(group):
         for d in range(1, nsp):
@@ -800,7 +802,7 @@
         for i in range(2):
             kt[i] = (dv_acc[0] if i else dk_acc[0] * score_scale).astype(BF16)
             key_copy(i).start()
-        lat_send(1)
+        lat_send(5)
 
     def return_keys():
         for i, acc, scale in ((0, dk_acc, score_scale), (1, dv_acc, 1.0)):
@@ -836,10 +838,12 @@
                 for h in range(pair):
                     out[:, p * pair + h, :] = kret[i, p, :, h * width : (h + 1) * width]
 
-    def query_results():
+    def query_results(own):
         for p in range(2):
-            for h in range(pair):
-                dq_out[:, p * pair + h, :] = db[z, p, half_of(y), h * width : (h + 1) * width]
+            @pl.when((y == p) if own else (y != p))
+            def _():
+                for h in range(pair):
+                    dq_out[:, p * pair + h, :] = db[z, p, half_of(y), h * width : (h + 1) * width]
 
     def weights(level):
         for c in range(2):
@@ -915,10 +919,12 @@
                 total_copy(j, half).start()
 
         key_total(0)
+        share_send(1)
         total(high)
+        share_hand(1)
         total(top)
         key_total(1)
-        lat_share(1)
+        lat_share(5)
 
     @pl.when(z == high)
     def _():
@@ -934,12 +940,13 @@
         total(high)
         lat_send(4)
         share_send(2)
+        share_send(1)
         key_results()
         share_hand(2)
+        share_hand(1)
         total(top)
         hand_on(0)
-        share_send(1)
-        share_hand(1)
+        lat_share(5)
 
     @pl.when(z < low)
     def _():
@@ -947,7 +954,9 @@
         hand_on(low)
         share_hand(0)
         share_send(1)
+        share_send(5)
         share_hand(1)
+        share_hand(5)
         share_send(3)
         share_hand(3)
 
@@ -958,45 +967,14 @@
         hand_on(low)
         share_hand(0)
         key_results()
+        share_send(1)
+        hand_on(high)
         lat_send(4)
-        hand_on(high)
+        share_hand(1)
         hand_on(top)
+        share_send(5)
         hand_on(0)
-        share_send(1)
-        share_hand(1)
-
-    own_lat().wait()
-    for level in range(high):
-        weights(level)
-
-        @pl.when(z < low)
-        def _():
-            hand_on(high + level)
-
-    @pl.when(z < high)
-    def _():
-        query_results()
-        share_send(4)
-
-        @pl.when(z == low)
-        def _():
-            key_results()
-
-        @pl.when(z < low)
-        def _():
-            key_results((0,))
-        share_hand(4)
-
-    for level in range(high, nz):
-        weights(level)
-
-        @pl.when(z == level)
-        def _():
-            query_results()
-
-    @pl.when(z < low)
-    def _():
-        key_results((1,))
+        share_hand(5)
 
     def sent(c):
         c.wait_send()
@@ -1011,8 +989,6 @@
         def _():
             for half in range(2):
                 sent(relay(a, half))
-    for level in range(nz):
-        grad_each(level, sent)
     for i in range(2):
         @pl.when(z >= low)
         def _():
@@ -1022,11 +998,6 @@
         def _():
             for c in range(2):
                 sent(part_copy(i, c))
-
-        @pl.when(z == low)
-        def _():
-            for half in range(2):
-                sent(total_copy(i, half))
 
         @pl.when(z < low)
         def _():
@@ -1038,6 +1009,57 @@
             sent(top_copy(c))
     for d in range(1, nsp):
         sent(lat_copy(d))
+
+    own_lat().wait()
+
+    @pl.when(z > high)
+    def _():
+        query_results(True)
+
+    for level in range(high):
+        weights(level)
+
+        @pl.when(z < low)
+        def _():
+            hand_on(high + level)
+
+    @pl.when(z < high)
+    def _():
+        query_results(True)
+        query_results(False)
+        share_send(4)
+
+        @pl.when(z == low)
+        def _():
+            key_results()
+
+        @pl.when(z < low)
+        def _():
+            key_results((0,))
+        share_hand(4)
+
+    for level in range(high, nz):
+        weights(level)
+
+        @pl.when(z == level)
+        def _():
+            if level < top:
+                query_results(True)
+            query_results(False)
+
+        if level == high:
+            @pl.when(z < low)
+            def _():
+                key_results((1,))
+
+    for level in range(nz):
+        grad_each(level, sent)
+
+    @pl.when(z == low)
+    def _():
+        for i in range(2):
+            for half in range(2):
+                sent(total_copy(i, half))
 
     def drain(d, carry):
         for k in range(2 * sides):

time: 75.8 us -> 73.4 us (0.968); the launches traced: 74.3 us -> 73.1 us
  Pallas kernels: 69 us -> 67.8 us
    pallas_call x1, Pallas kernels: 67.7 us -> 66.5 us  [hub_body(): pl.pallas_call(functools.partial(hub_kernel, nsp, ntp, heads, width), out...]
where the time goes in v5:
time: 73.4 us; the launch traced here: 73.1 us
  Pallas kernels  67.8 us (92%)
  other arithmetic  2.41 us (3%)
  local copies, waits for them, and re-layouts  2.08 us (3%)
  between operations  0.83 us (1%)
    pallas_call x1, Pallas kernels, hub_body(): pl.pallas_call(functools.partial(hub_kernel, nsp, ntp, heads, width), out...  66.5 us
    concatenate x1, other arithmetic, hub_body(): jnp.concatenate([map_outputs, out_grad[:, None]], axis=1)  1.67 us

profile of v5, /device:TPU:0, one launch (start us, length us, event | category | flops | bytes accessed | tf_op | source)
XLA Modules:
  0.0 73.1 jit_solution(14739388806242969027)
XLA Ops:
  0.6 0.7 %pad_add_fusion.small = f32[5,2,256]{2,1,0:T(2,128)S(1)} fusion(f32[1,1,4]{2,1,0:T(1,128)} %bitcast.20, f32[1,1,128]{2,1,0:T(1,128)} %bitcast.21, f32[4,2,256]{2,1,0:T(2,128)} %bitcast.19), kind=kLoop, calls=%fused_computation.4 | loop fusion | flops 5120 | bytes 18960 | tf_op jit(solution)/shard_map/add | solution.py:1101
  1.4 1.0 %copy.19 = bf16[32,8,4,128]{3,1,2,0:T(8,128)(2,1)S(1)} copy(bf16[32,8,4,128]{3,2,1,0:T(4,128)(2,1)} %bitcast.15) | data formatting | bytes 524288
  2.4 1.1 %copy_bitcast_fusion = (bf16[256,512]{1,0:T(8,128)(2,1)S(1)}, bf16[256,512]{1,0:T(8,128)(2,1)S(1)}) fusion(bf16[32,8,4,128]{3,2,1,0:T(4,128)(2,1)} %bitcast.16, bf16[32,8,4,128]{3,2,1,0:T(4,128)(2,1)} %bitcast.17), kind=kLoop, calls=%fused_computation.1 | loop fusion | bytes 1048576 | tf_op jit(solution)/shard_map/reshape | solution.py:1145
  3.5 1.7 %pad_maximum_fusion.maps = bf16[256,3,4,128]{3,2,1,0:T(4,128)(2,1)S(1)} fusion(bf16[256,1,4,128]{3,2,1,0:T(4,128)(2,1)} %bitcast.18, bf16[256,2,4,128]{3,2,1,0:T(4,128)(2,1)} %param.13), kind=kLoop, calls=%fused_computation | loop fusion | flops 393216 | bytes 1572864 | tf_op jit(solution)/shard_map/concatenate | solution.py:1146
  5.1 66.5 %hub.1 = (bf16[256,4,128]{2,1,0:T(4,128)(2,1)S(1)}, bf16[256,4,128]{2,1,0:T(4,128)(2,1)S(1)}, bf16[256,4,128]{2,1,0:T(4,128)(2,1)S(1)}, f32[512,512]{1,0:T(8,128)S(1)}) custom-call(f32[5,2,256]{2,1,0:T(2,128)S(1)} %pad_add_fusion.small, bf16[256,4096]{1,0:T(8,128)(2,1)} %lat.1, bf16[256,512]{1,0:T(8,128)(2,1)S(1)} %bitcast.14, ...), custom_call_target="tpu_custom_call" | custom-call | tf_op jit(solution)/shard_map/hub/pallas_call | solution.py:1105
  71.7 1.3 %finish.1 = (bf16[256,4,128]{2,1,0:T(4,128)(2,1)}, bf16[256,4,128]{2,1,0:T(4,128)(2,1)}, bf16[256,4,128]{2,1,0:T(4,128)(2,1)}, f32[512,512]{1,0:T(8,128)}) custom-call(bf16[256,4,128]{2,1,0:T(4,128)(2,1)S(1)} %get-tuple-element.8.a, bf16[256,4,128]{2,1,0:T(4,128)(2,1)S(1)} %get-tuple-element.9.b, bf16[256,4,128]{2,1,0:T(4,128)(2,1)S(1)} %get-tuple-element.10.c, ...), custom_call_target="tpu_custom_call" | custom-call | tf_op jit(solution)/shard_map/finish/pallas_call | solution.py:1148

commit v6 on v5

--- a/solution.py
+++ b/solution.py
@@ -924,7 +924,9 @@
         share_hand(1)
         total(top)
         key_total(1)
-        lat_share(5)
+        share_send(5)
+        share_send(4)
+        share_hand(5)
 
     @pl.when(z == high)
     def _():
@@ -1027,7 +1029,10 @@
     def _():
         query_results(True)
         query_results(False)
-        share_send(4)
+
+        @pl.when(z < low)
+        def _():
+            share_send(4)
 
         @pl.when(z == low)
         def _():

time: 73.4 us -> 73.4 us (level)
  no operation moved by 1% of the time
where the time goes in v6:
time: 73.4 us; the launch traced here: 73.1 us
  Pallas kernels  67.8 us (92%)
  other arithmetic  2.41 us (3%)
  local copies, waits for them, and re-layouts  2.08 us (3%)
  between operations  0.83 us (1%)
    pallas_call x1, Pallas kernels, hub_body(): pl.pallas_call(functools.partial(hub_kernel, nsp, ntp, heads, width), out...  66.5 us
    concatenate x1, other arithmetic, hub_body(): jnp.concatenate([map_outputs, out_grad[:, None]], axis=1)  1.67 us

profile of v6, /device:TPU:0, one launch (start us, length us, event | category | flops | bytes accessed | tf_op | source)
XLA Modules:
  0.0 73.1 jit_solution(11937216381962707145)
XLA Ops:
  0.6 0.7 %pad_add_fusion.small = f32[5,2,256]{2,1,0:T(2,128)S(1)} fusion(f32[1,1,4]{2,1,0:T(1,128)} %bitcast.20, f32[1,1,128]{2,1,0:T(1,128)} %bitcast.21, f32[4,2,256]{2,1,0:T(2,128)} %bitcast.19), kind=kLoop, calls=%fused_computation.4 | loop fusion | flops 5120 | bytes 18960 | tf_op jit(solution)/shard_map/add | solution.py:1106
  1.4 1.0 %copy.19 = bf16[32,8,4,128]{3,1,2,0:T(8,128)(2,1)S(1)} copy(bf16[32,8,4,128]{3,2,1,0:T(4,128)(2,1)} %bitcast.15) | data formatting | bytes 524288
  2.4 1.1 %copy_bitcast_fusion = (bf16[256,512]{1,0:T(8,128)(2,1)S(1)}, bf16[256,512]{1,0:T(8,128)(2,1)S(1)}) fusion(bf16[32,8,4,128]{3,2,1,0:T(4,128)(2,1)} %bitcast.16, bf16[32,8,4,128]{3,2,1,0:T(4,128)(2,1)} %bitcast.17), kind=kLoop, calls=%fused_computation.1 | loop fusion | bytes 1048576 | tf_op jit(solution)/shard_map/reshape | solution.py:1150
  3.5 1.7 %pad_maximum_fusion.maps = bf16[256,3,4,128]{3,2,1,0:T(4,128)(2,1)S(1)} fusion(bf16[256,1,4,128]{3,2,1,0:T(4,128)(2,1)} %bitcast.18, bf16[256,2,4,128]{3,2,1,0:T(4,128)(2,1)} %param.13), kind=kLoop, calls=%fused_computation | loop fusion | flops 393216 | bytes 1572864 | tf_op jit(solution)/shard_map/concatenate | solution.py:1151
  5.1 66.5 %hub.1 = (bf16[256,4,128]{2,1,0:T(4,128)(2,1)S(1)}, bf16[256,4,128]{2,1,0:T(4,128)(2,1)S(1)}, bf16[256,4,128]{2,1,0:T(4,128)(2,1)S(1)}, f32[512,512]{1,0:T(8,128)S(1)}) custom-call(f32[5,2,256]{2,1,0:T(2,128)S(1)} %pad_add_fusion.small, bf16[256,4096]{1,0:T(8,128)(2,1)} %lat.1, bf16[256,512]{1,0:T(8,128)(2,1)S(1)} %bitcast.14, ...), custom_call_target="tpu_custom_call" | custom-call | tf_op jit(solution)/shard_map/hub/pallas_call | solution.py:1110
  71.7 1.3 %finish.1 = (bf16[256,4,128]{2,1,0:T(4,128)(2,1)}, bf16[256,4,128]{2,1,0:T(4,128)(2,1)}, bf16[256,4,128]{2,1,0:T(4,128)(2,1)}, f32[512,512]{1,0:T(8,128)}) custom-call(bf16[256,4,128]{2,1,0:T(4,128)(2,1)S(1)} %get-tuple-element.8.a, bf16[256,4,128]{2,1,0:T(4,128)(2,1)S(1)} %get-tuple-element.9.b, bf16[256,4,128]{2,1,0:T(4,128)(2,1)S(1)} %get-tuple-element.10.c, ...), custom_call_target="tpu_custom_call" | custom-call | tf_op jit(solution)/shard_map/finish/pallas_call | solution.py:1153
